TPU v7x, 512 devices: a whole 4x4x16 slice. The times are simulated.
512 devices in a mesh: fs: 64 (over z, y), tp: 8 (over x, core).
Axes of the slice: x: 4, y: 4, z: 16, core: 2. Of those that a mesh axis runs over, the one named last changes fastest.
Arguments:
- tokens: bfloat16 [16384, 2048], P('fs'), may hold values from -6 to 6
- mix_gain: float32 [2048], replicated, may hold values from 0.1 to 1.9
- glu_value: bfloat16 [2048, 2048], P('fs', 'tp'), may hold values from -0.125 to 0.125
- glu_gate: bfloat16 [2048, 2048], P('fs', 'tp'), may hold values from -0.125 to 0.125
- conv_taps: float32 [31, 2048], P(None, 'tp'), may hold values from -2.2 to 2.2, as said below
- chan_gain: float32 [2048], P('tp'), may hold values from 0.1 to 1.9
- mix_out: bfloat16 [2048, 2048], P('tp', 'fs'), may hold values from -0.125 to 0.125
- mlp_gain: float32 [2048], replicated, may hold values from 0.1 to 1.9
- up_weight: bfloat16 [2048, 8192], P('fs', 'tp'), may hold values from -0.125 to 0.125
- down_weight: bfloat16 [8192, 2048], P('tp', 'fs'), may hold values from -0.0625 to 0.0625
Outputs:
- result: bfloat16 [16384, 2048], P('fs')
Inputs may be any that keep to these rules, and one draw needn't show every extreme that they name: `conv_taps`: independent entries scaled by fan-in; channels fall into 16 groups of different scale.
All inputs are finite; a program needn't handle non-finite values.
Results may differ from a plain program's by a relative error of at most 0.018.
Values may be sent and summed in bfloat16 or wider, within the bound.
A program may use at most 64 MiB of HBM per device.

v0:
```python
import jax
import jax.numpy as jnp
from jax import lax
from jax.sharding import PartitionSpec as P

C = 2048
LEN = 128


norm_floor = 0.05


def in_one_piece(arrays, axis, dim, along):
    widths = [a.shape[along] for a in arrays]
    both = jnp.concatenate(arrays, axis=along)
    result = lax.all_gather(both, axis, axis=dim, tiled=True)
    return tuple(jnp.split(result, [sum(widths[:k]) for k in range(1, len(widths))], axis=along))


def rows_first(arrays, axis, dims):
    turned = [jnp.moveaxis(a, dim, 0) for a, dim in zip(arrays, dims)]
    both = jnp.concatenate([t.reshape(len(t), -1) for t in turned], axis=1)
    result, at, gathered = (lax.all_gather(both, axis, axis=0, tiled=True), 0, [])
    for t, dim in zip(turned, dims):
        piece = result[:, at : at + t[0].size].reshape(-1, *t.shape[1:])
        gathered.append(jnp.moveaxis(piece, 0, dim))
        at += t[0].size
    return tuple(gathered)


def sent_to_all(shard, axis):
    count = lax.axis_size(axis)
    return lax.all_to_all(
        jnp.broadcast_to(shard[None], (count, *shard.shape)), axis, 0, 0, tiled=True
    )


def over_copies(shard, axis):
    everything = sent_to_all(shard, axis)
    return jnp.sum(everything, axis=0)


def together(arrays, axis):
    vector, at, gathered = (jnp.concatenate([a.reshape(-1) for a in arrays]), 0, [])
    running = over_copies(vector, axis)
    for a in arrays:
        gathered.append(running[at : at + a.size].reshape(a.shape))
        at += a.size
    return tuple(gathered)


def in_blocks(shard, dim, count):
    shape = shard.shape
    pieces = shard.reshape(*shape[:dim], count, shape[dim] // count, *shape[dim + 1 :])
    return jnp.moveaxis(pieces, dim, 0)


def summed_on_arrival(shard, axis, dim):
    count = lax.axis_size(axis)
    pieces = lax.all_to_all(in_blocks(shard, dim, count), axis, 0, 0, tiled=True)
    return jnp.sum(pieces.astype(jnp.float32), axis=0)


def joined_along(pieces, dim):
    shape = list(pieces.shape[1:])
    shape[dim] *= pieces.shape[0]
    return jnp.moveaxis(pieces, 0, dim).reshape(shape)


def gather_directly(shard, axis, dim):
    return joined_along(sent_to_all(shard, axis), dim)


def rms_scale(stream, gain):
    return stream * lax.rsqrt(jnp.mean(stream * stream, axis=-1, keepdims=True) + norm_floor) * gain


def bf16_round(value):
    return lax.optimization_barrier(value.astype(jnp.bfloat16)).astype(jnp.float32)


def depthwise(glu, conv_taps):
    seqs = glu.shape[0] // LEN
    blocks = glu.reshape(seqs, LEN, glu.shape[1]).astype(jnp.float32)
    reach = conv_taps.shape[0] // 2
    padded = jnp.pad(blocks, ((0, 0), (reach, reach), (0, 0)))
    total = jnp.zeros_like(blocks)
    for offset in range(conv_taps.shape[0]):
        total = total + padded[:, offset : offset + LEN] * conv_taps[offset]
    return total.reshape(glu.shape)


def per_device(
    tokens,
    mix_gain,
    glu_value,
    glu_gate,
    conv_taps,
    chan_gain,
    mix_out,
    mlp_gain,
    up_weight,
    down_weight,
):
    stream = tokens.astype(jnp.float32)
    normed = rms_scale(stream, mix_gain).astype(jnp.bfloat16)
    row_parts = in_one_piece((glu_value, glu_gate, up_weight), "fs", 0, 1)
    column_parts = rows_first((mix_out, down_weight), "fs", (1, 1))
    values = jnp.dot(normed, row_parts[0], preferred_element_type=jnp.float32)
    gating = jnp.dot(normed, row_parts[1], preferred_element_type=jnp.float32)
    glu = (values * jax.nn.sigmoid(gating)).astype(jnp.bfloat16)
    convolved = depthwise(glu, conv_taps)
    sums, squares = together(
        (jnp.sum(convolved, axis=-1), jnp.sum(convolved * convolved, axis=-1)), "tp"
    )
    centre = (sums / C)[:, None]
    spread = (squares / C)[:, None] - centre * centre
    hidden = jax.nn.silu((convolved - centre) * lax.rsqrt(spread + norm_floor) * chan_gain).astype(
        jnp.bfloat16
    )
    whole_out = column_parts[0]
    own_rows = stream.shape[0] // lax.axis_size("tp")
    mixed = summed_on_arrival(
        jnp.dot(hidden, whole_out, preferred_element_type=jnp.float32).astype(jnp.bfloat16), "tp", 0
    )
    own_stream = lax.dynamic_slice_in_dim(stream, lax.axis_index("tp") * own_rows, own_rows, 0)
    resid = own_stream + bf16_round(mixed)
    normed_mlp = rms_scale(resid, mlp_gain).astype(jnp.bfloat16)
    whole_up = row_parts[2]
    active = jnp.square(
        jax.nn.relu(
            jnp.dot(
                gather_directly(normed_mlp, "tp", 0), whole_up, preferred_element_type=jnp.float32
            )
        )
    ).astype(jnp.bfloat16)
    whole_down = column_parts[1]
    feed = summed_on_arrival(
        jnp.dot(active, whole_down, preferred_element_type=jnp.float32).astype(jnp.bfloat16),
        "tp",
        0,
    )
    finished = (resid + bf16_round(feed)).astype(jnp.bfloat16)
    return gather_directly(finished, "tp", 0)


def solution(mesh):
    in_specs = (
        P("fs", None),
        P(),
        P("fs", "tp"),
        P("fs", "tp"),
        P(None, "tp"),
        P("tp"),
        P("tp", "fs"),
        P(),
        P("fs", "tp"),
        P("tp", "fs"),
    )
    out_specs = P("fs", None)
    return jax.shard_map(
        per_device, mesh=mesh, in_specs=in_specs, out_specs=out_specs, check_vma=False
    )
```

profile of v0, /device:TPU:1, one launch (start us, length us, event | category | flops | bytes accessed | tf_op | source)
XLA Modules:
  0.0 408.4 jit_solution(4157544092094613481)
XLA Ops:
  6.5 1.5 pad_maximum_fusion
  8.0 0.0 all-gather.3.cloned.1.call-update
  8.1 0.0 all-gather.5.cloned.1.call-start
  8.1 1.5 pad_maximum_fusion.1
  9.6 0.0 all-gather.5.cloned.1.call-update
  9.6 1.5 multiply_reduce_fusion
  11.1 0.0 copy-start.3
  11.2 1.0 fusion.94
  12.1 1.0 fusion.93
  13.2 145.1 %all-gather.3.cloned.1.call-done = bf16[2048,1536]{1,0:T(8,128)(2,1)} async-done(((bf16[32,1536]{1,0:T(8,128)(2,1)}), bf16[2048,1536]{1,0:T(8,128)(2,1)}) %all-gather.3.cloned.1.call-update) | async-done | bytes 6291472 | tf_op jit(solution)/shard_map/all_gather | solution.py:16
  158.3 2.0 fusion.23
  160.4 1.8 bitcast_convert_fusion
  162.1 1.2 fusion.91
  163.3 17.4 %all_to_all.26 = f32[8,1,512]{2,1,0:T(1,128)S(1)} all-to-all(f32[8,1,512]{2,1,0:T(1,128)S(1)} %broadcast_in_dim.6), channel_id=1, replica_groups=mesh['fs'=64,'tp'=8] {'tp'}, dimensions={0} | all-to-all | bytes 32768 | tf_op jit(solution)/shard_map/all_to_all | solution.py:33
  180.8 0.2 multiply_convert_fusion.4
  181.0 123.2 %all-gather.5.cloned.1.call-done = bf16[2048,1280]{1,0:T(8,128)(2,1)} async-done(((bf16[32,1280]{1,0:T(8,128)(2,1)}), bf16[2048,1280]{1,0:T(8,128)(2,1)}) %all-gather.5.cloned.1.call-update) | async-done | bytes 5242896 | tf_op jit(solution)/shard_map/all_gather | solution.py:23
  304.2 2.7 convolution_convert_fusion
  306.9 14.1 %all-to-all-start.1 = ((bf16[8,32,2048]{2,1,0:T(8,128)(2,1)}), bf16[8,32,2048]{2,1,0:T(8,128)(2,1)S(1)}, u32[]{:S(2)}, u32[]{:S(2)}) async-start(bf16[8,32,2048]{2,1,0:T(8,128)(2,1)} %bitcast.38), calls=%async_computation.1 | async-start | bytes 2097152 | tf_op jit(solution)/shard_map/all_to_all | solution.py:60
  320.9 1.7 convert_element_type.45
  322.6 13.3 %all-to-all-done.1 = bf16[8,32,2048]{2,1,0:T(8,128)(2,1)S(1)} async-done(((bf16[8,32,2048]{2,1,0:T(8,128)(2,1)}), bf16[8,32,2048]{2,1,0:T(8,128)(2,1)S(1)}, u32[]{:S(2)}, u32[]{:S(2)}) %all-to-all-start.1) | async-done | bytes 1048608 | tf_op jit(solution)/shard_map/all_to_all | solution.py:60
  335.9 0.1 reduce_sum.79
  336.1 1.1 multiply_reduce_fusion.1
  337.2 1.0 multiply_convert_fusion.3
  338.2 0.1 broadcast_in_dim.7
  338.4 18.3 %all_to_all.27 = bf16[8,32,2048]{2,1,0:T(8,128)(2,1)S(1)} all-to-all(bf16[8,32,2048]{2,1,0:T(8,128)(2,1)S(1)} %broadcast_in_dim.7), channel_id=1, replica_groups=mesh['fs'=64,'tp'=8] {'tp'}, dimensions={0} | all-to-all | bytes 2097152 | tf_op jit(solution)/shard_map/all_to_all | solution.py:33
  356.7 5.8 %fusion.4 = bf16[256,2048]{1,0:T(8,128)(2,1)S(1)} fusion(bf16[2048,1280]{1,0:T(8,128)(2,1)} %all-gather.5.cloned.1.call-done, bf16[256,2048]{1,0:T(8,128)(2,1)S(1)} %bitcast.53, bf16[2048,1536]{1,0:T(8,128)(2,1)} %all-gather.3.cloned.1.call-done), kind=kOutput, calls=%fused_computation.4 | convolution fusion | flops 2148794368 | bytes 10485760 | tf_op jit(solution)/shard_map/dot_general | solution.py:139
  362.5 18.4 %all_to_all.28 = bf16[8,32,2048]{2,1,0:T(8,128)(2,1)S(1)} all-to-all(bf16[8,32,2048]{2,1,0:T(8,128)(2,1)S(1)} %bitcast.54), channel_id=1, replica_groups=mesh['fs'=64,'tp'=8] {'tp'}, dimensions={0} | all-to-all | bytes 2097152 | tf_op jit(solution)/shard_map/all_to_all | solution.py:60
  380.9 0.1 reduce_sum.81
  381.0 1.0 add_convert_fusion
  382.0 0.1 broadcast_in_dim.8
  382.2 18.4 %all_to_all.29 = bf16[8,32,2048]{2,1,0:T(8,128)(2,1)S(1)} all-to-all(bf16[8,32,2048]{2,1,0:T(8,128)(2,1)S(1)} %broadcast_in_dim.8), channel_id=1, replica_groups=mesh['fs'=64,'tp'=8] {'tp'}, dimensions={0} | all-to-all | bytes 2097152 | tf_op jit(solution)/shard_map/all_to_all | solution.py:33
  400.6 1.0 copy.16
  (14 shorter events, 0.1 us)
Async XLA Ops:
  6.5 151.8 %all-gather.3.cloned.1.call-start = ((), (), s32[]{:S(2)}) async-start(), calls=%async_computation.5 | async-start | bytes 6389760 | tf_op jit(solution)/shard_map/all_gather | solution.py:16
  8.1 296.2 %all-gather.5.cloned.1.call-start = ((), (), s32[]{:S(2)}) async-start(), calls=%async_computation.6 | async-start | bytes 5324800 | tf_op jit(solution)/shard_map/all_gather | solution.py:23
  11.1 149.2 %copy-start = (bf16[256,2048]{1,0:T(8,128)(2,1)S(1)}, bf16[256,2048]{1,0:T(8,128)(2,1)}, u32[]{:S(2)}) copy-start(bf16[256,2048]{1,0:T(8,128)(2,1)} %param.10) | copy-start | bytes 3145732
  11.1 149.2 %copy-start.3 = (f32[2048]{0:T(1024)S(1)}, f32[2048]{0:T(1024)}, u32[]{:S(2)}) copy-start(f32[2048]{0:T(1024)} %param.11) | copy-start | bytes 24580
  160.4 20.4 %copy-start.2 = (f32[256]{0:T(256)S(1)}, f32[256]{0:T(256)}, u32[]{:S(2)}) copy-start(f32[256]{0:T(256)} %param.15) | copy-start | bytes 3076
  306.9 29.0 %all-to-all-start.1 = ((bf16[8,32,2048]{2,1,0:T(8,128)(2,1)}), bf16[8,32,2048]{2,1,0:T(8,128)(2,1)S(1)}, u32[]{:S(2)}, u32[]{:S(2)}) async-start(bf16[8,32,2048]{2,1,0:T(8,128)(2,1)} %bitcast.38), calls=%async_computation.1 | async-start | bytes 2097152 | tf_op jit(solution)/shard_map/all_to_all | solution.py:60
  320.9 16.2 %copy-start.1 = (f32[2048]{0:T(1024)S(1)}, f32[2048]{0:T(1024)}, u32[]{:S(2)}) copy-start(f32[2048]{0:T(1024)} %param.17) | copy-start | bytes 24580
Sparse Core Ops, SparseCore 0:
  10.3 147.9 all-gather.2
  161.2 142.9 all-gather.4
where the time goes:
time: 409 us; the launch traced here: 408 us
  waiting for transfers between devices  282 us (69%)
  blocking collectives  72.5 us (18%)
  starting transfers between devices  14.1 us (3%)
  between operations  13.5 us (3%)
  matrix products  12.3 us (3%)
  other arithmetic  11 us (3%)
    all_gather x1, waiting for transfers between devices, in_one_piece(): result = lax.all_gather(both, axis, axis=dim, tiled=True)  145 us
    all_gather x1, waiting for transfers between devices, rows_first(): lax.all_gather(both, axis, axis=0, tiled=True)  123 us
    all_to_all x3, blocking collectives, sent_to_all(): lax.all_to_all(jnp.broadcast_to(shard[None], (count, *shard.shape)), axis...  54.1 us
    all_to_all x1, blocking collectives, summed_on_arrival(): lax.all_to_all(in_blocks(shard, dim, count), axis, 0, 0, tiled=True)  18.4 us
    all_to_all x1, starting transfers between devices, summed_on_arrival(): lax.all_to_all(in_blocks(shard, dim, count), axis, 0, 0, tiled=True)  14.1 us
    all_to_all x1, waiting for transfers between devices, summed_on_arrival(): lax.all_to_all(in_blocks(shard, dim, count), axis, 0, 0, tiled=True)  13.3 us
  transfers between devices with their start and end apart: 3, of which 3 were waited for; matrix products, arithmetic and copies ran while one was open for 3% of the time, Pallas kernels for 0%

commit v1 on v0

v1 whole, which is shorter than its diff:
```python
import functools

import jax
import jax.numpy as jnp
from jax import lax
from jax.experimental import pallas as pl
from jax.experimental.pallas import tpu as pltpu
from jax.sharding import PartitionSpec as P

MESH = pl.DeviceIdType.MESH
LEN = 128
NY = 4
FLOOR = 0.05
f32, bf16 = jnp.float32, jnp.bfloat16

GROUPS = ((0, 1, 2, 3), (4, 5, 6), (7, 8))


def copy_to(src, dst, ssem, rsem, dev):
    return pltpu.make_async_remote_copy(
        src_ref=src, dst_ref=dst, send_sem=ssem, recv_sem=rsem, device_id=dev, device_id_type=MESH
    )


class Place:
    def __init__(self, nfs):
        self.f, self.t = lax.axis_index("fs"), lax.axis_index("tp")
        self.nz = nfs // NY
        self.half = self.nz // 2
        self.z, self.y = self.f // NY, lax.rem(self.f, NY)

    def blk(self, dz, dy):
        z = lax.rem(self.z + (dz + self.nz), self.nz)
        return z * NY + lax.rem(self.y + (dy + NY), NY)

    def row(self, dz):
        return lax.rem(self.z + (dz + self.nz), self.nz)

    def dev(self, dz, dy):
        return (self.blk(dz, dy), self.t)

    def shifts(self, k):
        if k == 0:
            return (0,)
        return (self.half,) if k == self.half else (-k, k)


class ZFirst:
    def __init__(self, pc, w, ss, zr, yr, hr):
        self.pc, self.w, self.ss, self.zr, self.yr, self.hr = pc, w, ss, zr, yr, hr
        self.n = w.shape[1] // 2

    def part(self, b, which):
        return self.w.at[b, pl.ds(which * self.n, self.n)]

    def send(self, ref, rsem, dev):
        copy_to(ref, ref, self.ss, rsem, dev).start()

    def wait(self, ref, rsem):
        copy_to(ref, ref, self.ss, rsem, self.pc.dev(1, 0)).wait_recv()

    def z(self, k):
        pc, last = self.pc, self.pc.half
        if k == last:
            for d in range(2):
                self.wait(self.part(pc.blk(last, 0), d), self.zr.at[d, k])
        elif k:
            self.wait(self.w.at[pc.blk(-k, 0)], self.zr.at[0, k])
            self.wait(self.w.at[pc.blk(k, 0)], self.zr.at[1, k])
        if k < last:
            for d, way in ((0, 1), (1, -1)):
                b = pc.blk(-way * k, 0)
                ref = self.w.at[b] if k + 1 < last else self.part(b, d)
                self.send(ref, self.zr.at[d, k + 1], pc.dev(way, 0))
        for dz in pc.shifts(k):
            for d, way in ((0, 1), (1, -1)):
                self.send(self.w.at[pc.blk(dz, 0)], self.yr.at[d, k], pc.dev(0, way))

    def f(self, k):
        pc, shifts = self.pc, self.pc.shifts(k)
        for d in range(2):
            self.wait(self.w.at[pl.ds(0, len(shifts))], self.yr.at[d, k])
        for dz in shifts:
            for d, way in ((0, 1), (1, -1)):
                self.send(self.part(pc.blk(dz, -way), d), self.hr.at[d, k], pc.dev(0, way))

    def e(self, k):
        count = len(self.pc.shifts(k))
        for d in range(2):
            if count == 2:
                self.wait(self.w.at[0], self.hr.at[d, k])
            else:
                self.wait(self.part(0, d), self.hr.at[d, k])

    def drain(self):
        whole = self.w.at[pl.ds(0, self.w.shape[0] - 1)]
        copy_to(whole, whole, self.ss, self.zr.at[0, 0], self.pc.dev(1, 0)).wait_send()


class YFirst:
    def __init__(self, pc, w, ss, zr, yr, hr):
        self.pc, self.w, self.ss, self.zr, self.yr, self.hr = pc, w, ss, zr, yr, hr
        self.n = w.shape[1] // 2

    part, send, wait, drain = ZFirst.part, ZFirst.send, ZFirst.wait, ZFirst.drain

    def y0(self):
        for d, way in ((0, 1), (1, -1)):
            self.send(self.w.at[self.pc.f], self.yr.at[d], self.pc.dev(0, way))

    def y1(self):
        pc = self.pc
        for d, way in ((0, 1), (1, -1)):
            b = pc.blk(0, -way)
            self.wait(self.w.at[b], self.yr.at[d])
            self.send(self.part(b, d), self.hr.at[d], pc.dev(0, way))

    def four(self, dz):
        return self.w.at[pl.ds(self.pc.row(dz) * NY, NY)]

    def two(self, dz, which):
        return self.w.at[pl.ds(self.pc.row(dz) * NY + which * 2, 2)]

    def z(self, k):
        pc, last = self.pc, self.pc.half
        if k == 0:
            for d in range(2):
                self.wait(self.part(pc.blk(0, 2), d), self.hr.at[d])
        for d, way in ((0, 1), (1, -1)):
            if k == last:
                self.wait(self.two(last, d), self.zr.at[d, k])
            elif k:
                self.wait(self.four(-way * k), self.zr.at[d, k])
            if k < last:
                ref = self.four(-way * k) if k + 1 < last else self.two(-way * k, d)
                self.send(ref, self.zr.at[d, k + 1], pc.dev(way, 0))


def level(zf, yf, j):
    last = zf.pc.half
    if j <= last:
        zf.z(j)
    if 1 <= j <= last + 1:
        zf.f(j - 1)
    if 2 <= j <= last + 2:
        zf.e(j - 2)
    if j == 0:
        yf.y0()
    if j == 1:
        yf.y1()
    if 2 <= j <= last + 2:
        yf.z(j - 2)


class Exchange:
    def __init__(self, pc, src, dst, sems, spread):
        self.pc, self.src, self.dst, self.sems, self.spread = pc, src, dst, sems, spread

    def start(self):
        pc = self.pc
        nt = self.dst.shape[0]
        for i in range(1, nt):
            to = lax.rem(pc.t + i, nt)
            src = self.src.at[pc.t] if self.spread else self.src.at[to]
            copy_to(src, self.dst.at[pc.t], self.sems.at[0], self.sems.at[1], (pc.f, to)).start()

    def wait(self):
        pc = self.pc
        n = self.dst.shape[0] - 1
        some = self.dst.at[pl.ds(0, n)]
        copy_to(some, some, self.sems.at[0], self.sems.at[1], (pc.f, lax.rem(pc.t + 1, n + 1))).wait_recv()

    def drain(self):
        pc = self.pc
        n = self.dst.shape[0] - 1
        some = self.dst.at[pl.ds(0, n)]
        copy_to(some, some, self.sems.at[0], self.sems.at[1], (pc.f, lax.rem(pc.t + 1, n + 1))).wait_send()


def nt_dot(a, b):
    return lax.dot_general(a, b, (((1,), (1,)), ((), ())), preferred_element_type=f32)


def turned(column):
    return jnp.broadcast_to(column, (column.shape[0], 128)).T[0:1]


def column_of(row):
    return jnp.broadcast_to(row, (128, row.shape[1])).T


def body(
    nfs,
    tok, mix_gain, vw, gw, taps, chan_gain, ow, mlp_gain, uw, dw,
    out,
    x, normed, q1, p1, uq, up, dq, dp,
    padded, conv, stats, mx, rx, nm, resid, aq, ap,
    fx, fr, og,
    load_sem, out_sem,
    q1_s, p1_s, uq_s, up_s, dq_s, dp_s,
    st_sem, mx_sem, nm_sem, fx_sem, og_sem,
):
    pc = Place(nfs)
    nt = rx.shape[0]
    rows = rx.shape[1]
    width = x.shape[1]
    tokens = x.shape[0]
    seqs = tokens // LEN
    last = pc.half
    wq, uc, dc = vw.shape[1], uq.shape[2], dq.shape[2]

    loads = [
        pltpu.make_async_copy(src, dst, load_sem.at[i])
        for i, (src, dst) in enumerate((
            (vw, q1.at[pc.f, :, pl.ds(0, wq)]),
            (gw, q1.at[pc.f, :, pl.ds(wq, wq)]),
            (ow, p1.at[pc.f]),
            (uw.at[:, pl.ds(0, uc)], uq.at[pc.f]),
            (uw.at[:, pl.ds(uc, uw.shape[1] - uc)], up.at[pc.f]),
            (dw.at[:, pl.ds(0, dc)], dq.at[pc.f]),
            (dw.at[:, pl.ds(dc, dw.shape[1] - dc)], dp.at[pc.f]),
            (tok, x),
        ))
    ]
    for load in loads:
        load.start()

    barrier = pltpu.get_barrier_semaphore()
    friends = [pc.dev(1, 0), pc.dev(-1, 0), pc.dev(0, 1), pc.dev(0, -1)]
    friends += [(pc.f, lax.rem(pc.t + i, nt)) for i in range(1, nt)]
    for dev in friends:
        pl.semaphore_signal(barrier, inc=1, device_id=dev, device_id_type=MESH)
    for load in loads:
        load.wait()
    pl.semaphore_wait(barrier, len(friends))

    glu_w, out_w = ZFirst(pc, q1, *q1_s), YFirst(pc, p1, *p1_s)
    up_z, up_y = ZFirst(pc, uq, *uq_s), YFirst(pc, up, *up_s)
    down_z, down_y = ZFirst(pc, dq, *dq_s), YFirst(pc, dp, *dp_s)

    def first(j):
        level(glu_w, out_w, j)

    def second(j):
        level(up_z, up_y, j)

    def third(j):
        level(down_z, down_y, j)

    first(0)
    second(0)

    def norm_rows(i, carry):
        at = pl.ds(pl.multiple_of(i * 32, 32), 32)
        s = x[at].astype(f32)
        scale = lax.rsqrt(jnp.mean(s * s, axis=-1, keepdims=True) + FLOOR)
        normed[at] = (s * scale * mix_gain[...]).astype(bf16)
        return carry

    lax.fori_loop(0, tokens // 32, norm_rows, 0)

    done = 1
    for j in range(1, last + 3):
        first(j)
        if j % 2 == 0 and done < 5:
            second(done)
            done += 1

    n_all = normed[...]
    values = jnp.dot(n_all, q1[:, :, pl.ds(0, wq)].reshape(width, wq), preferred_element_type=f32)
    gating = jnp.dot(n_all, q1[:, :, pl.ds(wq, wq)].reshape(width, wq), preferred_element_type=f32)
    glu = (values * jax.nn.sigmoid(gating)).astype(bf16).astype(f32)
    reach = taps.shape[0] // 2
    halves = wq // 128
    zeros = jnp.zeros((16, 128), f32)
    for h in range(halves):
        for s in range(seqs):
            padded[h, s, pl.ds(0, 16)] = zeros
            padded[h, s, pl.ds(16, LEN)] = glu[s * LEN : (s + 1) * LEN, h * 128 : (h + 1) * 128]
            padded[h, s, pl.ds(16 + LEN, 16)] = zeros
    second(done)
    third(0)

    for h in range(halves):
        for s in range(seqs):
            total = jnp.zeros((LEN, 128), f32)
            for o in range(taps.shape[0]):
                total = total + padded[h, s, pl.ds(16 - reach + o, LEN)] * taps[pl.ds(o, 1), pl.ds(h * 128, 128)]
            conv[h, pl.ds(s * LEN, LEN)] = total
    sums = sum(jnp.sum(conv[h], axis=-1, keepdims=True) for h in range(halves))
    squares = sum(jnp.sum(conv[h] * conv[h], axis=-1, keepdims=True) for h in range(halves))
    stats[pc.t, pl.ds(0, 1)] = turned(sums)
    stats[pc.t, pl.ds(1, 1)] = turned(squares)
    second(done + 1)
    stat_x = Exchange(pc, stats, stats, st_sem, True)
    stat_x.start()
    third(1)
    stat_x.wait()

    all_stats = jnp.sum(stats[...], axis=0)
    channels = wq * nt
    centre = column_of(all_stats[0:1]) / channels
    spread = column_of(all_stats[1:2]) / channels - centre * centre
    scale = lax.rsqrt(spread + FLOOR)
    hidden = []
    for h in range(halves):
        v = (conv[h] - centre) * scale * chan_gain[:, h * 128 : (h + 1) * 128]
        hidden.append((v * jax.nn.sigmoid(v)).astype(bf16))
    hidden = jnp.concatenate(hidden, axis=1)
    for c in range(width // 256):
        w = p1[pl.ds(c * 8, 8)].reshape(256, wq)
        mx[:, :, pl.ds(c * 256, 256)] = nt_dot(hidden, w).astype(bf16).reshape(nt, rows, 256)
    second(done + 2)
    mix_x = Exchange(pc, mx, rx, mx_sem, False)
    mix_x.start()
    third(2)
    second(done + 3)
    third(3)
    mix_x.wait()

    rx[pc.t] = mx[pc.t]
    mixed = rx[0].astype(f32)
    for i in range(1, nt):
        mixed = mixed + rx[i].astype(f32)
    own = x[pl.ds(pl.multiple_of(pc.t * rows, rows), rows)].astype(f32)
    res = own + mixed.astype(bf16).astype(f32)
    resid[...] = res
    scale = lax.rsqrt(jnp.mean(res * res, axis=-1, keepdims=True) + FLOOR)
    nm[pc.t] = (res * scale * mlp_gain[...]).astype(bf16)
    second(done + 4)
    norm_x = Exchange(pc, nm, nm, nm_sem, True)
    norm_x.start()
    third(4)
    second(done + 5)
    third(5)
    norm_x.wait()

    n_mlp = nm[...].reshape(tokens, width)
    for src, dst in ((uq, aq), (up, ap)):
        cols = src.shape[2]
        for c in range(0, cols, 256):
            n = min(256, cols - c)
            a = jnp.dot(n_mlp, src[:, :, pl.ds(c, n)].reshape(width, n), preferred_element_type=f32)
            a = jnp.maximum(a, 0.0)
            dst[:, pl.ds(c, n)] = (a * a).astype(bf16)

    act_q, act_p = aq[...], ap[...]

    def slots(g):
        return [dz for k in GROUPS[g] for dz in pc.shifts(k)]

    def multiply(g):
        for s, dz in enumerate(slots(g)):
            b = pl.ds(pc.row(dz) * NY, NY)
            part = nt_dot(act_q, dq[b].reshape(128, dc)) + nt_dot(act_p, dp[b].reshape(128, dp.shape[2]))
            fx[g][:, :, pl.ds(s * 128, 128)] = part.astype(bf16).reshape(nt, rows, 128)

    sums_x = [Exchange(pc, fx[g], fr[g], fx_sem.at[g], False) for g in range(len(GROUPS))]
    done_x = [Exchange(pc, og[g], og[g], og_sem.at[g], True) for g in range(len(GROUPS))]

    def finish(g):
        sums_x[g].wait()
        fr[g][pc.t] = fx[g][pc.t]
        for s, dz in enumerate(slots(g)):
            at = pl.ds(s * 128, 128)
            feed = fr[g][0, :, at].astype(f32)
            for i in range(1, nt):
                feed = feed + fr[g][i, :, at].astype(f32)
            to = pl.ds(pl.multiple_of(pc.row(dz) * 128, 128), 128)
            og[g][pc.t, :, at] = (resid[:, to] + feed.astype(bf16).astype(f32)).astype(bf16)

    def write(g):
        done_x[g].wait()
        for s, dz in enumerate(slots(g)):
            to = pl.ds(pl.multiple_of(pc.row(dz) * 128, 128), 128)
            pltpu.make_async_copy(og[g].at[:, :, pl.ds(s * 128, 128)], out.at[:, :, to], out_sem).start()

    multiply(0)
    third(6)
    sums_x[0].start()
    third(7)
    third(8)
    multiply(1)
    sums_x[1].start()
    finish(0)
    done_x[0].start()
    third(9)
    third(10)
    multiply(2)
    sums_x[2].start()
    finish(1)
    done_x[1].start()
    write(0)
    finish(2)
    done_x[2].start()
    write(1)
    write(2)

    for stream in (glu_w, out_w, up_z, up_y, down_z, down_y):
        stream.drain()
    for x_ in [stat_x, mix_x, norm_x, *sums_x, *done_x]:
        x_.drain()
    pltpu.make_async_copy(out, out, out_sem).wait()


def layer(nfs, nt, tok, mix_gain, vw, gw, taps, chan_gain, ow, mlp_gain, uw, dw):
    tokens, width = tok.shape
    k_rows, wq = vw.shape
    ff = uw.shape[1]
    rows = tokens // nt
    last = nfs // NY // 2
    uc = ff * 5 // 8
    dma = pltpu.SemaphoreType.DMA
    one = lambda: [dma(()), dma((2, last + 1)), dma((2, last + 1)), dma((2, last + 1))]
    other = lambda: [dma(()), dma((2, last + 1)), dma((2,)), dma((2,))]
    widths = [sum(1 if k in (0, last) else 2 for k in g) * 128 for g in GROUPS]
    pieces = lambda: [pltpu.VMEM((nt, rows, w), bf16) for w in widths]
    block = lambda c: pltpu.VMEM((nfs, k_rows, c), bf16)
    hbm, vmem = pl.BlockSpec(memory_space=pl.ANY), pl.BlockSpec(memory_space=pltpu.VMEM)
    scratch = [
        pltpu.VMEM((tokens, width), bf16),
        pltpu.VMEM((tokens, width), bf16),
        block(2 * wq), block(wq), block(uc), block(ff - uc), block(uc), block(ff - uc),
        pltpu.VMEM((wq // 128, tokens // LEN, LEN + 32, 128), f32),
        pltpu.VMEM((wq // 128, tokens, 128), f32),
        pltpu.VMEM((nt, 2, tokens), f32),
        pltpu.VMEM((nt, rows, width), bf16),
        pltpu.VMEM((nt, rows, width), bf16),
        pltpu.VMEM((nt, rows, width), bf16),
        pltpu.VMEM((rows, width), f32),
        pltpu.VMEM((tokens, uc), bf16),
        pltpu.VMEM((tokens, ff - uc), bf16),
        pieces(), pieces(), pieces(),
        dma((8,)), dma(()),
        one(), other(), one(), other(), one(), other(),
        dma((2,)), dma((2,)), dma((2,)), dma((len(GROUPS), 2)), dma((len(GROUPS), 2)),
    ]
    done = pl.pallas_call(
        functools.partial(body, nfs),
        out_shape=jax.ShapeDtypeStruct((nt, rows, width), bf16),
        in_specs=[hbm, vmem, hbm, hbm, vmem, vmem, hbm, vmem, hbm, hbm],
        out_specs=hbm,
        scratch_shapes=scratch,
        compiler_params=pltpu.CompilerParams(
            collective_id=0, has_side_effects=True, vmem_limit_bytes=56 * 1024 * 1024
        ),
        name="layer",
    )(
        tok, mix_gain.reshape(1, -1), vw, gw, taps, chan_gain.reshape(1, -1), ow.T,
        mlp_gain.reshape(1, -1), uw, dw.T,
    )
    return done.reshape(tokens, width)


def solution(mesh):
    in_specs = (
        P("fs", None), P(), P("fs", "tp"), P("fs", "tp"), P(None, "tp"),
        P("tp"), P("tp", "fs"), P(), P("fs", "tp"), P("tp", "fs"),
    )
    nfs, nt = mesh.shape["fs"], mesh.shape["tp"]
    return jax.shard_map(
        functools.partial(layer, nfs, nt), mesh=mesh, in_specs=in_specs,
        out_specs=P("fs", None), check_vma=False,
    )
```

time: 409 us -> 129 us (0.32)
  waiting for transfers between devices: 282 us -> 0 us
  Pallas kernels: 0 us -> 126 us
  blocking collectives: 72.5 us -> 0 us
  starting transfers between devices: 14.1 us -> 0 us
  between operations: 13.5 us -> 0.01 us
  matrix products: 12.3 us -> 0 us
  other arithmetic: 11 us -> 0 us
    all_gather x2 -> x0, waiting for transfers between devices: 268 us -> none  [the longest x1 145 us: in_one_piece(): result = lax.all_gather(both, axis, axis=dim, tiled=True)]
    pallas_call x0 -> x1, Pallas kernels: none -> 126 us  [layer(): pl.pallas_call(functools.partial(body, nfs), out_shape=jax.ShapeDtypeStru...]
    all_to_all x4 -> x0, blocking collectives: 72.5 us -> none  [the longest x3 54.1 us: sent_to_all(): lax.all_to_all(jnp.broadcast_to(shard[None], (count, *shard.shape)), axis...]
    all_to_all x1 -> x0, starting transfers between devices: 14.1 us -> none  [summed_on_arrival(): lax.all_to_all(in_blocks(shard, dim, count), axis, 0, 0, tiled=True)]
    all_to_all x1 -> x0, waiting for transfers between devices: 13.3 us -> none  [summed_on_arrival(): lax.all_to_all(in_blocks(shard, dim, count), axis, 0, 0, tiled=True)]
    dot_general x4 -> x0, matrix products: 12.3 us -> none  [the longest x1 5.81 us: per_device(): jnp.dot(active, whole_down, preferred_element_type=jnp.float32)]
    reduce_sum x6 -> x0, other arithmetic: 4.12 us -> none  [the longest x2 2.61 us: rms_scale(): jnp.mean(stream * stream, axis=-1, keepdims=True) + norm_floor]
  transfers between devices with their start and end apart: 3 -> 0, of which waited for: 3 -> 0; matrix products, arithmetic and copies ran while one was open for 3% -> 0% of each run, Pallas kernels for 0% -> 0%
where the time goes in v1:
time: 129 us
  Pallas kernels  126 us (98%)
  local copies, waits for them, and re-layouts  2.3 us (2%)
    pallas_call x1, Pallas kernels, layer(): pl.pallas_call(functools.partial(body, nfs), out_shape=jax.ShapeDtypeStru...  126 us

profile of v1, /device:TPU:1, one launch (start us, length us, event | category | flops | bytes accessed | tf_op | source)
XLA Modules:
  0.0 128.5 jit_solution(7100330167187441264)
XLA Ops:
  0.0 126.2 %layer.1 = bf16[8,32,2048]{2,1,0:T(8,128)(2,1)} custom-call(bf16[256,2048]{1,0:T(8,128)(2,1)} %tok.1, f32[1,2048]{1,0:T(1,128)} %bitcast.9, bf16[32,256]{1,0:T(8,128)(2,1)} %vw.1, bf16[32,256]{1,0:T(8,128)(2,1)} %gw.1, f32[31,256]{1,0:T(8,128)} %taps.1, f32[1,256]{1,0:T(1,128)} %bitcast.11, bf16[32,256]{1,0:T(8,128)(2,1)} %bitcast.8, f32[1,2048]{1,0:T(1,128)} %bitcast.10, ...), custom_call_target="tpu_custom_call" | custom-call | tf_op jit(solution)/shard_map/layer/pallas_call | solution.py:438
  126.2 2.3 %copy.12 = bf16[256,2048]{1,0:T(8,128)(2,1)} copy(bf16[256,2048]{1,0:T(8,128)(2,1)} %bitcast.6) | data formatting | bytes 2097152

commit v2 on v0

v2 whole, which is shorter than its diff:
```python
import functools

import jax
import jax.numpy as jnp
from jax import lax
from jax.experimental import pallas as pl
from jax.experimental.pallas import tpu as pltpu
from jax.sharding import PartitionSpec as P

MESH = pl.DeviceIdType.MESH
LEN = 128
NY = 4
FLOOR = 0.05
f32, bf16 = jnp.float32, jnp.bfloat16

ORDER = (
    "v.y0", "g.z0", "u.z0", "d.y0", "e.y0", "o.y0", "o.z0", "d.z0", "g.y0", "u.y0", "g.z1", "v.y1", "g.y1", "g.y2",
    "o.y1", "g.z2", "u.y1", "e.y1", "u.f0", "g.f0", "o.z1", "o.z2", "o.f0", "g.z3", "g.y3", "d.z1", "g.z4", "u.f1",
    "u.z1", "o.y3", "o.y4", "v.z01", "o.z4", "o.z3", "d.y2", "g.f1", "v.z00", "g.y5", "d.z2", "u.z2", "g.z6", "g.z5",
    "o.y2", "v.z11", "g.y6", "d.f0", "g.y4", "o.f4", "d.z3", "o.z6", "v.z10", "o.z5", "g.f2", "d.f2", "g.y8", "u.z3",
    "o.f1", "g.y7", "o.y6", "e.z01", "o.y5", "v.z20", "e.z00", "N", "g.f4", "u.z4", "g.f3", "e.z11", "g.f6", "g.f5",
    "o.f2", "o.y8", "o.f6", "d.z4", "d.y3", "o.y7", "e.z10", "u.z5", "o.f5", "o.f3", "v.z21", "u.y5", "v.z30", "u.y4",
    "G", "e.z21", "C", "u.y2", "e.z20", "v.z31", "v.z40", "H", "u.y3", "d.y1", "d.z5", "u.z6", "I", "B", "v.z41",
    "v.z50", "u.f4", "d.y5", "d.f3", "u.z7", "e.z30", "u.y7", "u.y6", "v.z51", "e.z31", "d.z6", "e.z40", "v.z60",
    "u.y8", "u.f5", "E", "e.z41", "d.y4", "u.f2", "v.z61", "e.z50", "u.f6", "u.f3", "d.f1", "e.z51", "v.z71", "v.z70",
    "d.f5", "d.z7", "e.z60", "d.f4", "d.y6", "L", "e.z61", "d.y7", "U", "M0", "d.f6", "d.y8", "M1", "e.z70", "e.z71",
    "S0", "S1", "M2", "M3", "S2", "S3", "F0", "F1", "F3", "F2", "R0", "W0", "R3", "R1", "R2", "W1", "W3", "W2",
)
GROUPS = ((0, 1, 2, 3), (4, 5), (6, 7), (8,))
DIRECT = 7


def copy_to(src, dst, ssem, rsem, dev):
    return pltpu.make_async_remote_copy(
        src_ref=src, dst_ref=dst, send_sem=ssem, recv_sem=rsem, device_id=dev, device_id_type=MESH
    )


class Place:
    def __init__(self, nfs, nt):
        self.f, self.t = lax.axis_index("fs"), lax.axis_index("tp")
        self.nz = nfs // NY
        self.half = self.nz // 2
        self.z, self.y = self.f // NY, lax.rem(self.f, NY)
        self.nx = nt // 2
        self.x, self.c = self.t // 2, lax.rem(self.t, 2)

    def row(self, dz):
        return lax.rem(self.z + (dz + self.nz), self.nz)

    def blk(self, dz, dy):
        return self.row(dz) * NY + lax.rem(self.y + (dy + NY), NY)

    def dev(self, dz, dy):
        return (self.blk(dz, dy), self.t)

    def along_x(self, i):
        x = lax.rem(self.x + i, self.nx)
        return x, (self.f, x * 2 + self.c)

    def partner(self):
        return (self.f, self.x * 2 + 1 - self.c)

    def shifts(self, k):
        if k == 0:
            return (0,)
        return (self.half,) if k == self.half else (-k, k)


class Stream:
    def __init__(self, pc, w, sems, loads, stride):
        self.pc, self.w, self.loads, self.stride = pc, w, loads, stride
        self.ss, self.zr, self.yr, self.hr = sems
        self.n = w.shape[1] // 2
        self.came = set()

    def part(self, b, which):
        return self.w.at[b, pl.ds(which * self.n, self.n)]

    def send(self, ref, rsem, dev):
        copy_to(ref, ref, self.ss, rsem, dev).start()

    def await_(self, ref, rsem):
        copy_to(ref, ref, self.ss, rsem, self.pc.dev(1, 0)).wait_recv()

    def need(self, *key):
        if key not in self.came:
            self.came.add(key)
            self.arrive(*key)

    def own(self):
        if "own" not in self.came:
            self.came.add("own")
            for load in self.loads:
                load.wait()

    def drain(self):
        whole = self.w.at[pl.ds(0, self.w.shape[0] - 1)]
        copy_to(whole, whole, self.ss, self.yr.at[0, 0], self.pc.dev(1, 0)).wait_send()


class ZFirst(Stream):
    def arrive(self, what, k):
        pc = self.pc
        for d in range(2):
            if what == "z":
                b = pc.blk(k if d else -k, 0)
                self.await_(self.part(b, d) if k == pc.half else self.w.at[b], self.zr.at[d, k])
            elif what == "y":
                self.await_(self.w.at[pl.ds(0, len(pc.shifts(k)))], self.yr.at[d, k])
            elif k >= DIRECT:
                if d == 0:
                    self.await_(self.w.at[pl.ds(0, len(pc.shifts(k)))], self.hr.at[0, k])
            else:
                self.await_(self.w.at[0] if len(pc.shifts(k)) == 2 else self.part(0, d), self.hr.at[d, k])

    def all_of(self, k):
        self.own()
        for what in "zyh" if k else "yh":
            self.need(what, k)

    def ready(self, k):
        if k:
            self.need("z", k)
        else:
            self.own()

    def z(self, k):
        pc = self.pc
        self.ready(k)
        for step in range(1, self.stride + 1) if k == 0 else (self.stride,):
            for d, way in ((0, 1), (1, -1)):
                b = pc.blk(-way * k, 0)
                ref = self.part(b, d) if k + step == pc.half else self.w.at[b]
                self.send(ref, self.zr.at[d, k + step], pc.dev(way * step, 0))

    def y(self, k):
        pc = self.pc
        self.ready(k)
        for dz in pc.shifts(k):
            ref = self.w.at[pc.blk(dz, 0)]
            for d, way in ((0, 1), (1, -1)):
                self.send(ref, self.yr.at[d, k], pc.dev(0, way))
            if k >= DIRECT:
                self.send(ref, self.hr.at[0, k], pc.dev(0, 2))

    def f(self, k):
        pc = self.pc
        self.need("y", k)
        for dz in pc.shifts(k):
            for d, way in ((0, 1), (1, -1)):
                self.send(self.part(pc.blk(dz, -way), d), self.hr.at[d, k], pc.dev(0, way))


class YFirst(Stream):
    def two(self, dz, h):
        return self.w.at[pl.ds(self.pc.row(dz) * NY + h * 2, 2)]

    def arrive(self, what, k, h=0):
        pc = self.pc
        for d, way in ((0, 1), (1, -1)):
            if what == "y":
                self.await_(self.w.at[pc.blk(0, -way)], self.yr.at[d, 0])
            elif what == "h":
                self.await_(self.part(pc.blk(0, 2), d), self.hr.at[d, 0])
            elif k < pc.half or d == h:
                self.await_(self.two(-way * k, h), self.zr.at[d, k, h])

    def all_of(self, k):
        self.own()
        if k:
            for h in range(2):
                self.need("z", k, h)
        else:
            self.need("y", 0)
            self.need("h", 0)

    def y(self, k):
        pc = self.pc
        if k == 0:
            self.own()
        else:
            self.need("y", 0)
        for d, way in ((0, 1), (1, -1)):
            if k == 0:
                self.send(self.w.at[pc.f], self.yr.at[d, 0], pc.dev(0, way))
            else:
                self.send(self.part(pc.blk(0, -way), d), self.hr.at[d, 0], pc.dev(0, way))

    def z(self, kh):
        pc = self.pc
        k, h = kh // 10, kh % 10
        if k:
            self.need("z", k, h)
        else:
            self.all_of(0)
        for d, way in ((0, 1), (1, -1)):
            if k + 1 < pc.half or d == h:
                self.send(self.two(-way * k, h), self.zr.at[d, k + 1, h], pc.dev(way, 0))


class PairSum:
    def __init__(self, pc, other, got, mine, came, sems):
        self.pc, self.other, self.got, self.mine, self.came, self.sems = pc, other, got, mine, came, sems

    def swap(self):
        return copy_to(self.other, self.got, self.sems.at[0], self.sems.at[1], self.pc.partner())

    def spread(self):
        pc = self.pc
        for i in range(1, pc.nx):
            x, dev = pc.along_x(i)
            copy_to(self.mine.at[x], self.came.at[pc.x], self.sems.at[2], self.sems.at[3], dev).start()

    def three(self):
        some = self.came.at[pl.ds(0, self.pc.nx - 1)]
        return copy_to(some, some, self.sems.at[2], self.sems.at[3], self.pc.partner())


class PairGather:
    def __init__(self, pc, buf, sems):
        self.pc, self.buf, self.sems = pc, buf, sems

    def own(self):
        pc = self.pc
        ref = self.buf.at[pc.x, pc.c]
        return copy_to(ref, ref, self.sems.at[2], self.sems.at[3], pc.partner())

    def start(self):
        pc = self.pc
        ref = self.buf.at[pc.x, pc.c]
        for i in range(1, pc.nx):
            copy_to(ref, ref, self.sems.at[0], self.sems.at[1], pc.along_x(i)[1]).start()
        self.own().start()

    def some(self, i):
        ref = self.buf.at[pl.ds(0, self.pc.nx - 1), 0]
        return copy_to(ref, ref, self.sems.at[i], self.sems.at[i + 1], self.pc.partner())

    def relay(self):
        pc = self.pc
        self.some(0).wait_recv()
        for i in range(1, pc.nx):
            ref = self.buf.at[pc.along_x(i)[0], pc.c]
            copy_to(ref, ref, self.sems.at[4], self.sems.at[5], pc.partner()).start()

    def wait(self):
        self.own().wait_recv()
        self.some(4).wait_recv()

    def drain(self):
        self.some(0).wait_send()
        self.own().wait_send()
        self.some(4).wait_send()


def nt_dot(a, b):
    return lax.dot_general(a, b, (((1,), (1,)), ((), ())), preferred_element_type=f32)


def turned(column):
    return jnp.broadcast_to(column, (column.shape[0], 128)).T[0:1]


def column_of(row):
    return jnp.broadcast_to(row, (128, row.shape[1])).T


def body(
    nfs, nt,
    tok, mix_gain, vw, gw, taps, chan_gain, ow, mlp_gain, uw, dw,
    out,
    x, normed, gb, ob, ub, vb, db, eb,
    padded, conv, stats, hid, mo, mp, mm, mr, nm, resid, aq, ap,
    fx, fp, fm, fr, og,
    load_sem, out_sem, sems, st_sem, mx_sem, nm_sem, fx_sem, og_sem,
):
    pc = Place(nfs, nt)
    rows, width, tokens = nm.shape[2], x.shape[1], x.shape[0]
    seqs = tokens // LEN
    last = pc.half
    wq, uc, dc = vw.shape[1], ub.shape[2], db.shape[2]
    halves = wq // 128
    reach = taps.shape[0] // 2

    def load(src, dst, i):
        copy = pltpu.make_async_copy(src, dst, load_sem.at[i])
        copy.start()
        return copy

    own = dict(
        g=[load(vw, gb.at[pc.f, :, pl.ds(0, wq)], 0), load(gw, gb.at[pc.f, :, pl.ds(wq, wq)], 1)],
        o=[load(ow, ob.at[pc.f], 2)],
        u=[load(uw.at[:, pl.ds(0, uc)], ub.at[pc.f], 3)],
        v=[load(uw.at[:, pl.ds(uc, uw.shape[1] - uc)], vb.at[pc.f], 4)],
        d=[load(dw.at[:, pl.ds(0, dc)], db.at[pc.f], 5)],
        e=[load(dw.at[:, pl.ds(dc, dw.shape[1] - dc)], eb.at[pc.f], 6)],
    )
    tok_load = load(tok, x, 7)

    barrier = pltpu.get_barrier_semaphore()
    friends = [pc.dev(dz, 0) for dz in (1, -1, 2, -2)] + [pc.dev(0, dy) for dy in (1, -1, 2)]
    friends += [(pc.f, lax.rem(pc.t + i, nt)) for i in range(1, nt)]
    for dev in friends:
        pl.semaphore_signal(barrier, inc=1, device_id=dev, device_id_type=MESH)
    own["g"][0].wait()
    own["g"].pop(0)
    pl.semaphore_wait(barrier, len(friends))

    stream = {
        name: kind(pc, w, sems[i], own[name], stride)
        for i, (name, kind, w, stride) in enumerate((
            ("g", ZFirst, gb, 2), ("o", ZFirst, ob, 2), ("u", ZFirst, ub, 1), ("v", YFirst, vb, 1),
            ("d", ZFirst, db, 1), ("e", YFirst, eb, 1),
        ))
    }
    mix_sum = PairSum(pc, mo.at[1 - pc.c], mp, mm, mr, mx_sem)
    norm_all = PairGather(pc, nm, nm_sem)
    feed_sum = [
        PairSum(pc, fx[g].at[1 - pc.c], fp[g], fm[g], fr[g], fx_sem.at[g]) for g in range(len(GROUPS))
    ]
    feed_all = [PairGather(pc, og[g], og_sem.at[g]) for g in range(len(GROUPS))]

    def stat_copy(i):
        to = lax.rem(pc.t + i, nt)
        return copy_to(stats.at[pc.t], stats.at[pc.t], st_sem.at[0], st_sem.at[1], (pc.f, to))

    def stat_all():
        some = stats.at[pl.ds(0, nt - 1)]
        return copy_to(some, some, st_sem.at[0], st_sem.at[1], pc.partner())

    def norm_in():
        tok_load.wait()

        def some_rows(i, carry):
            at = pl.ds(pl.multiple_of(i * 32, 32), 32)
            s = x[at].astype(f32)
            scale = lax.rsqrt(jnp.mean(s * s, axis=-1, keepdims=True) + FLOOR)
            normed[at] = (s * scale * mix_gain[...]).astype(bf16)
            return carry

        lax.fori_loop(0, tokens // 32, some_rows, 0)

    def glu():
        for k in range(last + 1):
            stream["g"].all_of(k)
        n_all = normed[...]
        values = jnp.dot(n_all, gb[:, :, pl.ds(0, wq)].reshape(width, wq), preferred_element_type=f32)
        gating = jnp.dot(n_all, gb[:, :, pl.ds(wq, wq)].reshape(width, wq), preferred_element_type=f32)
        glued = (values * jax.nn.sigmoid(gating)).astype(bf16).astype(f32)
        zeros = jnp.zeros((16, 128), f32)
        for h in range(halves):
            for s in range(seqs):
                padded[h, s, pl.ds(0, 16)] = zeros
                padded[h, s, pl.ds(16, LEN)] = glued[s * LEN : (s + 1) * LEN, h * 128 : (h + 1) * 128]
                padded[h, s, pl.ds(16 + LEN, 16)] = zeros

    def convolve():
        for h in range(halves):
            for s in range(seqs):
                total = jnp.zeros((LEN, 128), f32)
                for o in range(taps.shape[0]):
                    tap = taps[pl.ds(o, 1), pl.ds(h * 128, 128)]
                    total = total + padded[h, s, pl.ds(16 - reach + o, LEN)] * tap
                conv[h, pl.ds(s * LEN, LEN)] = total
        sums = sum(jnp.sum(conv[h], axis=-1, keepdims=True) for h in range(halves))
        squares = sum(jnp.sum(conv[h] * conv[h], axis=-1, keepdims=True) for h in range(halves))
        stats[pc.t, pl.ds(0, 1)] = turned(sums)
        stats[pc.t, pl.ds(1, 1)] = turned(squares)
        for i in range(1, nt):
            stat_copy(i).start()

    def mix_rows(core):
        left = hid[:, core].reshape(tokens // 2, wq)
        for c in range(width // 256):
            w = ob[pl.ds(c * 8, 8)].reshape(256, wq)
            mo[core, :, :, pl.ds(c * 256, 256)] = nt_dot(left, w).astype(bf16).reshape(pc.nx, rows, 256)

    def channel_norm():
        stat_all().wait_recv()
        all_stats = jnp.sum(stats[...], axis=0)
        channels = wq * nt
        centre = column_of(all_stats[0:1]) / channels
        spread = column_of(all_stats[1:2]) / channels - centre * centre
        scale = lax.rsqrt(spread + FLOOR)
        for h in range(halves):
            at = pl.ds(h * 128, 128)
            v = (conv[h] - centre) * scale * chan_gain[:, at]
            hid[:, :, :, at] = (v * jax.nn.sigmoid(v)).astype(bf16).reshape(pc.nx, 2, rows, 128)
        for k in range(last + 1):
            stream["o"].all_of(k)
        mix_rows(1 - pc.c)
        mix_sum.swap().start()

    def mix_pair():
        mix_sum.swap().wait_recv()
        for i in range(pc.nx):
            mm[i] = (mo[pc.c, i].astype(f32) + mp[i].astype(f32)).astype(bf16)
        mix_sum.spread()

    def norm_mid():
        mix_sum.three().wait_recv()
        mr[pc.x] = mm[pc.x]
        mixed = sum(mr[i].astype(f32) for i in range(pc.nx))
        mine = x[pl.ds(pl.multiple_of(pc.t * rows, rows), rows)].astype(f32)
        res = mine + mixed.astype(bf16).astype(f32)
        resid[...] = res
        scale = lax.rsqrt(jnp.mean(res * res, axis=-1, keepdims=True) + FLOOR)
        nm[pc.x, pc.c] = (res * scale * mlp_gain[...]).astype(bf16)
        norm_all.start()

    def up():
        norm_all.wait()
        for k in range(last + 1):
            stream["u"].all_of(k)
            stream["v"].all_of(k)
        n_mlp = nm[...].reshape(tokens, width)
        for src, dst in ((ub, aq), (vb, ap)):
            cols = src.shape[2]
            for c in range(0, cols, 256):
                n = min(256, cols - c)
                a = jnp.dot(n_mlp, src[:, :, pl.ds(c, n)].reshape(width, n), preferred_element_type=f32)
                a = jnp.maximum(a, 0.0)
                dst[:, pl.ds(c, n)] = (a * a).astype(bf16)

    def slots(g):
        return [dz for k in GROUPS[g] for dz in pc.shifts(k)]

    def down(g):
        for k in GROUPS[g]:
            stream["d"].all_of(k)
            stream["e"].all_of(k)
        left = jnp.concatenate([aq[...], ap[...]], axis=1)
        for s, dz in enumerate(slots(g)):
            b = pl.ds(pc.row(dz) * NY, NY)
            part = nt_dot(left[:, :dc], db[b].reshape(128, dc))
            part = part + nt_dot(left[:, dc:], eb[b].reshape(128, eb.shape[2]))
            part = part.astype(bf16).reshape(pc.nx, 2, rows, 128)
            for core in range(2):
                fx[g][core, :, :, pl.ds(s * 128, 128)] = part[:, core]
        feed_sum[g].swap().start()

    def feed_pair(g):
        feed_sum[g].swap().wait_recv()
        for i in range(pc.nx):
            fm[g][i] = (fx[g][pc.c, i].astype(f32) + fp[g][i].astype(f32)).astype(bf16)
        feed_sum[g].spread()

    def finish(g):
        feed_sum[g].three().wait_recv()
        fr[g][pc.x] = fm[g][pc.x]
        for s, dz in enumerate(slots(g)):
            at = pl.ds(s * 128, 128)
            feed = sum(fr[g][i, :, at].astype(f32) for i in range(pc.nx))
            to = pl.ds(pl.multiple_of(pc.row(dz) * 128, 128), 128)
            og[g][pc.x, pc.c, :, at] = (resid[:, to] + feed.astype(bf16).astype(f32)).astype(bf16)
        feed_all[g].start()

    def write(g):
        feed_all[g].wait()
        for s, dz in enumerate(slots(g)):
            to = pl.ds(pl.multiple_of(pc.row(dz) * 128, 128), 128)
            pltpu.make_async_copy(og[g].at[:, :, :, pl.ds(s * 128, 128)], out.at[:, :, :, to], out_sem).start()

    steps = dict(
        N=norm_in, G=glu, C=convolve, H=channel_norm, I=lambda: mix_rows(pc.c), B=mix_pair, E=norm_mid,
        L=norm_all.relay, U=up,
    )
    by_group = dict(M=down, S=feed_pair, F=finish, R=lambda g: feed_all[g].relay(), W=write)
    for name in ORDER:
        if "." in name:
            getattr(stream[name[0]], name[2])(int(name[3:]))
        elif name in steps:
            steps[name]()
        else:
            by_group[name[0]](int(name[1:]))

    for s in stream.values():
        s.drain()
    stat_all().wait_send()
    for s in [mix_sum, *feed_sum]:
        s.swap().wait_send()
        s.three().wait_send()
    for s in [norm_all, *feed_all]:
        s.drain()
    pltpu.make_async_copy(out, out, out_sem).wait()


def layer(nfs, nt, tok, mix_gain, vw, gw, taps, chan_gain, ow, mlp_gain, uw, dw):
    tokens, width = tok.shape
    k_rows, wq = vw.shape
    ff = uw.shape[1]
    rows, nx = tokens // nt, nt // 2
    last = nfs // NY // 2
    uc, dc = ff * 5 // 8, ff // 2
    dma = pltpu.SemaphoreType.DMA
    z_first = lambda: [dma(()), dma((2, last + 1)), dma((2, last + 1)), dma((2, last + 1))]
    y_first = lambda: [dma(()), dma((2, last + 1, 2)), dma((2, 1)), dma((2, 1))]
    widths = [sum(1 if k in (0, last) else 2 for k in g) * 128 for g in GROUPS]
    block = lambda c: pltpu.VMEM((nfs, k_rows, c), bf16)
    pairs = lambda w: pltpu.VMEM((2, nx, rows, w), bf16)
    four = lambda w: pltpu.VMEM((nx, rows, w), bf16)
    eight = lambda w: pltpu.VMEM((nx, 2, rows, w), bf16)
    hbm, vmem = pl.BlockSpec(memory_space=pl.ANY), pl.BlockSpec(memory_space=pltpu.VMEM)
    scratch = [
        pltpu.VMEM((tokens, width), bf16),
        pltpu.VMEM((tokens, width), bf16),
        block(2 * wq), block(wq), block(uc), block(ff - uc), block(dc), block(ff - dc),
        pltpu.VMEM((wq // 128, tokens // LEN, LEN + 32, 128), f32),
        pltpu.VMEM((wq // 128, tokens, 128), f32),
        pltpu.VMEM((nt, 2, tokens), f32),
        eight(wq),
        pairs(width), four(width), four(width), four(width),
        eight(width),
        pltpu.VMEM((rows, width), f32),
        pltpu.VMEM((tokens, uc), bf16),
        pltpu.VMEM((tokens, ff - uc), bf16),
        [pairs(w) for w in widths], [four(w) for w in widths], [four(w) for w in widths],
        [four(w) for w in widths], [eight(w) for w in widths],
        dma((8,)), dma(()),
        [z_first(), z_first(), z_first(), y_first(), z_first(), y_first()],
        dma((2,)), dma((4,)), dma((6,)), dma((len(GROUPS), 4)), dma((len(GROUPS), 6)),
    ]
    done = pl.pallas_call(
        functools.partial(body, nfs, nt),
        out_shape=jax.ShapeDtypeStruct((nx, 2, rows, width), bf16),
        in_specs=[hbm, vmem, hbm, hbm, vmem, vmem, hbm, vmem, hbm, hbm],
        out_specs=hbm,
        scratch_shapes=scratch,
        compiler_params=pltpu.CompilerParams(
            collective_id=0, has_side_effects=True, vmem_limit_bytes=56 * 1024 * 1024
        ),
        name="layer",
    )(
        tok, mix_gain.reshape(1, -1), vw, gw, taps, chan_gain.reshape(1, -1), ow.T,
        mlp_gain.reshape(1, -1), uw, dw.T,
    )
    return done.reshape(tokens, width)


def solution(mesh):
    in_specs = (
        P("fs", None), P(), P("fs", "tp"), P("fs", "tp"), P(None, "tp"),
        P("tp"), P("tp", "fs"), P(), P("fs", "tp"), P("tp", "fs"),
    )
    nfs, nt = mesh.shape["fs"], mesh.shape["tp"]
    return jax.shard_map(
        functools.partial(layer, nfs, nt), mesh=mesh, in_specs=in_specs,
        out_specs=P("fs", None), check_vma=False,
    )
```

time: 409 us -> 106 us (0.26)
  waiting for transfers between devices: 282 us -> 0 us
  Pallas kernels: 0 us -> 103 us
  blocking collectives: 72.5 us -> 0 us
  starting transfers between devices: 14.1 us -> 0 us
  between operations: 13.5 us -> 0.01 us
  matrix products: 12.3 us -> 0 us
  other arithmetic: 11 us -> 0 us
    all_gather x2 -> x0, waiting for transfers between devices: 268 us -> none  [the longest x1 145 us: in_one_piece(): result = lax.all_gather(both, axis, axis=dim, tiled=True)]
    pallas_call x0 -> x1, Pallas kernels: none -> 103 us  [layer(): pl.pallas_call(functools.partial(body, nfs, nt), out_shape=jax.ShapeDtype...]
    all_to_all x4 -> x0, blocking collectives: 72.5 us -> none  [the longest x3 54.1 us: sent_to_all(): lax.all_to_all(jnp.broadcast_to(shard[None], (count, *shard.shape)), axis...]
    all_to_all x1 -> x0, starting transfers between devices: 14.1 us -> none  [summed_on_arrival(): lax.all_to_all(in_blocks(shard, dim, count), axis, 0, 0, tiled=True)]
    all_to_all x1 -> x0, waiting for transfers between devices: 13.3 us -> none  [summed_on_arrival(): lax.all_to_all(in_blocks(shard, dim, count), axis, 0, 0, tiled=True)]
    dot_general x4 -> x0, matrix products: 12.3 us -> none  [the longest x1 5.81 us: per_device(): jnp.dot(active, whole_down, preferred_element_type=jnp.float32)]
    reduce_sum x6 -> x0, other arithmetic: 4.12 us -> none  [the longest x2 2.61 us: rms_scale(): jnp.mean(stream * stream, axis=-1, keepdims=True) + norm_floor]
  transfers between devices with their start and end apart: 3 -> 0, of which waited for: 3 -> 0; matrix products, arithmetic and copies ran while one was open for 3% -> 0% of each run, Pallas kernels for 0% -> 0%
where the time goes in v2:
time: 106 us; the launch traced here: 105 us
  Pallas kernels  103 us (97%)
  local copies, waits for them, and re-layouts  2.3 us (2%)
    pallas_call x1, Pallas kernels, layer(): pl.pallas_call(functools.partial(body, nfs, nt), out_shape=jax.ShapeDtype...  103 us
    unnamed x1, local copies, waits for them, and re-layouts  2.3 us

profile of v2, /device:TPU:1, one launch (start us, length us, event | category | flops | bytes accessed | tf_op | source)
XLA Modules:
  0.0 105.3 jit_solution(11223832577204973601)
XLA Ops:
  0.0 103.0 %layer.1 = bf16[4,2,32,2048]{3,2,1,0:T(8,128)(2,1)} custom-call(bf16[256,2048]{1,0:T(8,128)(2,1)} %tok.1, f32[1,2048]{1,0:T(1,128)} %bitcast.9, bf16[32,256]{1,0:T(8,128)(2,1)} %vw.1, bf16[32,256]{1,0:T(8,128)(2,1)} %gw.1, f32[31,256]{1,0:T(8,128)} %taps.1, f32[1,256]{1,0:T(1,128)} %bitcast.11, bf16[32,256]{1,0:T(8,128)(2,1)} %bitcast.8, ...), custom_call_target="tpu_custom_call" | custom-call | tf_op jit(solution)/shard_map/layer/pallas_call | solution.py:524
  103.0 2.3 %copy.12 = bf16[256,2048]{1,0:T(8,128)(2,1)} copy(bf16[256,2048]{1,0:T(8,128)(2,1)} %bitcast.6) | data formatting | bytes 2097152

commit v3 on v2

--- a/solution.py
+++ b/solution.py
@@ -14,20 +14,23 @@
 f32, bf16 = jnp.float32, jnp.bfloat16
 
 ORDER = (
-    "v.y0", "g.z0", "u.z0", "d.y0", "e.y0", "o.y0", "o.z0", "d.z0", "g.y0", "u.y0", "g.z1", "v.y1", "g.y1", "g.y2",
-    "o.y1", "g.z2", "u.y1", "e.y1", "u.f0", "g.f0", "o.z1", "o.z2", "o.f0", "g.z3", "g.y3", "d.z1", "g.z4", "u.f1",
-    "u.z1", "o.y3", "o.y4", "v.z01", "o.z4", "o.z3", "d.y2", "g.f1", "v.z00", "g.y5", "d.z2", "u.z2", "g.z6", "g.z5",
-    "o.y2", "v.z11", "g.y6", "d.f0", "g.y4", "o.f4", "d.z3", "o.z6", "v.z10", "o.z5", "g.f2", "d.f2", "g.y8", "u.z3",
-    "o.f1", "g.y7", "o.y6", "e.z01", "o.y5", "v.z20", "e.z00", "N", "g.f4", "u.z4", "g.f3", "e.z11", "g.f6", "g.f5",
-    "o.f2", "o.y8", "o.f6", "d.z4", "d.y3", "o.y7", "e.z10", "u.z5", "o.f5", "o.f3", "v.z21", "u.y5", "v.z30", "u.y4",
-    "G", "e.z21", "C", "u.y2", "e.z20", "v.z31", "v.z40", "H", "u.y3", "d.y1", "d.z5", "u.z6", "I", "B", "v.z41",
-    "v.z50", "u.f4", "d.y5", "d.f3", "u.z7", "e.z30", "u.y7", "u.y6", "v.z51", "e.z31", "d.z6", "e.z40", "v.z60",
-    "u.y8", "u.f5", "E", "e.z41", "d.y4", "u.f2", "v.z61", "e.z50", "u.f6", "u.f3", "d.f1", "e.z51", "v.z71", "v.z70",
-    "d.f5", "d.z7", "e.z60", "d.f4", "d.y6", "L", "e.z61", "d.y7", "U", "M0", "d.f6", "d.y8", "M1", "e.z70", "e.z71",
-    "S0", "S1", "M2", "M3", "S2", "S3", "F0", "F1", "F3", "F2", "R0", "W0", "R3", "R1", "R2", "W1", "W3", "W2",
+    "o.y0", "o.z0", "e.y0", "g.z0", "g.y0", "u.y0", "d.y0", "u.z0", "o.y1", "o.z1", "g.z1", "v.y0", "g.y1", "g.z2",
+    "g.y2", "g.f0", "o.z2", "v.y1", "u.z1", "o.y2", "g.z3", "g.y3", "N", "g.f1", "o.z3", "g.z4", "v.z00", "g.f2",
+    "g.y4", "o.y3", "g.z5", "g.y5", "o.z4", "g.f3", "g.z6", "u.z2", "e.y1", "g.y6", "v.z01", "g.y7", "d.z0", "o.z5",
+    "v.z10", "g.y8", "g.f4", "u.z3", "g.f5", "v.z11", "g.f6", "o.z6", "e.z00", "g.f7", "g.f8", "d.z1", "o.y5", "o.f0",
+    "o.y6", "o.y4", "o.f2", "v.z20", "o.y7", "u.y3", "o.z7", "e.z01", "G", "v.z21", "o.f5", "u.z4", "o.y8", "d.z2",
+    "u.y2", "e.z10", "o.f7", "o.f6", "v.z30", "o.f1", "C", "o.f3", "o.f4", "o.f8", "u.f3", "u.y5", "u.z5", "v.z31",
+    "u.y1", "u.y4", "d.z3", "e.z11", "v.z40", "H", "u.y6", "v.z41", "I", "u.f2", "u.z6", "B0", "u.f5", "e.z21",
+    "v.z50", "B1", "v.z51", "u.y7", "e.z20", "u.z7", "u.f4", "E0", "u.f6", "u.f0", "d.z4", "d.y2", "v.z60", "v.z61",
+    "E1", "e.z30", "u.y8", "d.z5", "d.y1", "u.f1", "e.z31", "v.z70", "L0", "u.f7", "u.f8", "v.z71", "d.f0", "d.f2",
+    "L1", "d.f1", "d.y4", "e.z40", "e.z41", "d.y3", "d.z6", "d.y6", "d.y5", "U", "e.z50", "M0", "d.f4", "e.z51",
+    "d.f3", "S0", "d.y7", "d.z7", "d.f6", "e.z60", "d.f5", "e.z61", "M1", "F0", "d.f7", "d.y8", "S1", "e.z70", "M2",
+    "e.z71", "S2", "M3", "S3", "M4", "F1", "F2", "R0", "F3", "F4", "W0", "R1", "R2", "W1", "R3", "W2", "W4", "W3",
 )
-GROUPS = ((0, 1, 2, 3), (4, 5), (6, 7), (8,))
-DIRECT = 7
+GROUPS = ((0, 1, 2), (3, 4), (5, 6), (7,), (8,))
+STRIDE = {'g': 2}
+DIRECT = {'d': 8}
+PARTS = 2
 
 
 def copy_to(src, dst, ssem, rsem, dev):
@@ -68,8 +71,8 @@
 
 
 class Stream:
-    def __init__(self, pc, w, sems, loads, stride):
-        self.pc, self.w, self.loads, self.stride = pc, w, loads, stride
+    def __init__(self, pc, w, sems, loads, stride, direct):
+        self.pc, self.w, self.loads, self.stride, self.direct = pc, w, loads, stride, direct
         self.ss, self.zr, self.yr, self.hr = sems
         self.n = w.shape[1] // 2
         self.came = set()
@@ -108,7 +111,7 @@
                 self.await_(self.part(b, d) if k == pc.half else self.w.at[b], self.zr.at[d, k])
             elif what == "y":
                 self.await_(self.w.at[pl.ds(0, len(pc.shifts(k)))], self.yr.at[d, k])
-            elif k >= DIRECT:
+            elif k >= self.direct:
                 if d == 0:
                     self.await_(self.w.at[pl.ds(0, len(pc.shifts(k)))], self.hr.at[0, k])
             else:
@@ -141,7 +144,7 @@
             ref = self.w.at[pc.blk(dz, 0)]
             for d, way in ((0, 1), (1, -1)):
                 self.send(ref, self.yr.at[d, k], pc.dev(0, way))
-            if k >= DIRECT:
+            if k >= self.direct:
                 self.send(ref, self.hr.at[0, k], pc.dev(0, 2))
 
     def f(self, k):
@@ -223,25 +226,25 @@
 
     def own(self):
         pc = self.pc
-        ref = self.buf.at[pc.x, pc.c]
+        ref = self.buf.at[pc.t]
         return copy_to(ref, ref, self.sems.at[2], self.sems.at[3], pc.partner())
 
     def start(self):
         pc = self.pc
-        ref = self.buf.at[pc.x, pc.c]
+        ref = self.buf.at[pc.t]
         for i in range(1, pc.nx):
             copy_to(ref, ref, self.sems.at[0], self.sems.at[1], pc.along_x(i)[1]).start()
         self.own().start()
 
     def some(self, i):
-        ref = self.buf.at[pl.ds(0, self.pc.nx - 1), 0]
+        ref = self.buf.at[pl.ds(0, self.pc.nx - 1)]
         return copy_to(ref, ref, self.sems.at[i], self.sems.at[i + 1], self.pc.partner())
 
     def relay(self):
         pc = self.pc
         self.some(0).wait_recv()
         for i in range(1, pc.nx):
-            ref = self.buf.at[pc.along_x(i)[0], pc.c]
+            ref = self.buf.at[pc.along_x(i)[0] * 2 + pc.c]
             copy_to(ref, ref, self.sems.at[4], self.sems.at[5], pc.partner()).start()
 
     def wait(self):
@@ -254,6 +257,22 @@
         self.some(4).wait_send()
 
 
+class Exchange:
+    def __init__(self, pc, piece, came, sems):
+        self.pc, self.piece, self.came, self.sems = pc, piece, came, sems
+
+    def start(self):
+        pc, nt = self.pc, self.pc.nx * 2
+        for i in range(1, nt):
+            to = lax.rem(pc.t + i, nt)
+            dst = self.came.at[pc.t]
+            copy_to(self.piece(to), dst, self.sems.at[0], self.sems.at[1], (pc.f, to)).start()
+
+    def rest(self):
+        some = self.came.at[pl.ds(0, self.pc.nx * 2 - 1)]
+        return copy_to(some, some, self.sems.at[0], self.sems.at[1], self.pc.partner())
+
+
 def nt_dot(a, b):
     return lax.dot_general(a, b, (((1,), (1,)), ((), ())), preferred_element_type=f32)
 
@@ -268,15 +287,16 @@
 
 def body(
     nfs, nt,
-    tok, mix_gain, vw, gw, taps, chan_gain, ow, mlp_gain, uw, dw,
+    tok, mix_gain_in, vw, gw, taps_in, chan_gain_in, ow, mlp_gain_in, uw, dw,
     out,
+    mix_gain, taps, chan_gain, mlp_gain,
     x, normed, gb, ob, ub, vb, db, eb,
     padded, conv, stats, hid, mo, mp, mm, mr, nm, resid, aq, ap,
     fx, fp, fm, fr, og,
-    load_sem, out_sem, sems, st_sem, mx_sem, nm_sem, fx_sem, og_sem,
+    load_sem, sems, st_sem, mx_sem, nm_sem, fx_sem, og_sem,
 ):
     pc = Place(nfs, nt)
-    rows, width, tokens = nm.shape[2], x.shape[1], x.shape[0]
+    rows, width, tokens = nm.shape[1], x.shape[1], x.shape[0]
     seqs = tokens // LEN
     last = pc.half
     wq, uc, dc = vw.shape[1], ub.shape[2], db.shape[2]
@@ -297,6 +317,12 @@
         e=[load(dw.at[:, pl.ds(dc, dw.shape[1] - dc)], eb.at[pc.f], 6)],
     )
     tok_load = load(tok, x, 7)
+    small = [
+        load(src, dst, 8 + i)
+        for i, (src, dst) in enumerate((
+            (mix_gain_in, mix_gain), (taps_in, taps), (chan_gain_in, chan_gain), (mlp_gain_in, mlp_gain),
+        ))
+    ]
 
     barrier = pltpu.get_barrier_semaphore()
     friends = [pc.dev(dz, 0) for dz in (1, -1, 2, -2)] + [pc.dev(0, dy) for dy in (1, -1, 2)]
@@ -308,29 +334,29 @@
     pl.semaphore_wait(barrier, len(friends))
 
     stream = {
-        name: kind(pc, w, sems[i], own[name], stride)
-        for i, (name, kind, w, stride) in enumerate((
-            ("g", ZFirst, gb, 2), ("o", ZFirst, ob, 2), ("u", ZFirst, ub, 1), ("v", YFirst, vb, 1),
-            ("d", ZFirst, db, 1), ("e", YFirst, eb, 1),
+        name: kind(pc, w, sems[i], own[name], STRIDE.get(name, 1), DIRECT.get(name, last + 1))
+        for i, (name, kind, w) in enumerate((
+            ("g", ZFirst, gb), ("o", ZFirst, ob), ("u", ZFirst, ub), ("v", YFirst, vb), ("d", ZFirst, db),
+            ("e", YFirst, eb),
         ))
     }
-    mix_sum = PairSum(pc, mo.at[1 - pc.c], mp, mm, mr, mx_sem)
-    norm_all = PairGather(pc, nm, nm_sem)
-    feed_sum = [
-        PairSum(pc, fx[g].at[1 - pc.c], fp[g], fm[g], fr[g], fx_sem.at[g]) for g in range(len(GROUPS))
+    part_rows = rows // PARTS
+    parts = [pl.ds(i * part_rows, part_rows) for i in range(PARTS)]
+    mix_sum = [
+        PairSum(pc, mo.at[1 - pc.c, :, p], mp.at[:, p], mm.at[:, p], mr.at[:, p], mx_sem.at[i])
+        for i, p in enumerate(parts)
     ]
-    feed_all = [PairGather(pc, og[g], og_sem.at[g]) for g in range(len(GROUPS))]
-
-    def stat_copy(i):
-        to = lax.rem(pc.t + i, nt)
-        return copy_to(stats.at[pc.t], stats.at[pc.t], st_sem.at[0], st_sem.at[1], (pc.f, to))
-
-    def stat_all():
-        some = stats.at[pl.ds(0, nt - 1)]
-        return copy_to(some, some, st_sem.at[0], st_sem.at[1], pc.partner())
+    norm_all = [PairGather(pc, nm.at[:, p], nm_sem.at[i]) for i, p in enumerate(parts)]
+    end = len(GROUPS) - 1
+    feed_sum = [PairSum(pc, fx[g].at[1 - pc.c], fp[g], fm[g], fr[g], fx_sem.at[g]) for g in range(end)]
+    feed_all = [PairGather(pc, og[g], og_sem.at[g]) for g in range(end)]
+    end_sum = Exchange(pc, lambda to: fx[end].at[lax.rem(to, 2), to // 2], fr[end], fx_sem.at[end])
+    end_all = Exchange(pc, lambda to: og[end].at[pc.t], og[end], og_sem.at[end])
+    stat_all = Exchange(pc, lambda to: stats.at[pc.t], stats, st_sem)
 
     def norm_in():
-        tok_load.wait()
+        for copy in (tok_load, *small):
+            copy.wait()
 
         def some_rows(i, carry):
             at = pl.ds(pl.multiple_of(i * 32, 32), 32)
@@ -367,8 +393,7 @@
         squares = sum(jnp.sum(conv[h] * conv[h], axis=-1, keepdims=True) for h in range(halves))
         stats[pc.t, pl.ds(0, 1)] = turned(sums)
         stats[pc.t, pl.ds(1, 1)] = turned(squares)
-        for i in range(1, nt):
-            stat_copy(i).start()
+        stat_all.start()
 
     def mix_rows(core):
         left = hid[:, core].reshape(tokens // 2, wq)
@@ -377,7 +402,7 @@
             mo[core, :, :, pl.ds(c * 256, 256)] = nt_dot(left, w).astype(bf16).reshape(pc.nx, rows, 256)
 
     def channel_norm():
-        stat_all().wait_recv()
+        stat_all.rest().wait_recv()
         all_stats = jnp.sum(stats[...], axis=0)
         channels = wq * nt
         centre = column_of(all_stats[0:1]) / channels
@@ -390,27 +415,31 @@
         for k in range(last + 1):
             stream["o"].all_of(k)
         mix_rows(1 - pc.c)
-        mix_sum.swap().start()
-
-    def mix_pair():
-        mix_sum.swap().wait_recv()
-        for i in range(pc.nx):
-            mm[i] = (mo[pc.c, i].astype(f32) + mp[i].astype(f32)).astype(bf16)
-        mix_sum.spread()
-
-    def norm_mid():
-        mix_sum.three().wait_recv()
-        mr[pc.x] = mm[pc.x]
-        mixed = sum(mr[i].astype(f32) for i in range(pc.nx))
-        mine = x[pl.ds(pl.multiple_of(pc.t * rows, rows), rows)].astype(f32)
-        res = mine + mixed.astype(bf16).astype(f32)
-        resid[...] = res
+        for m in mix_sum:
+            m.swap().start()
+
+    def mix_pair(i):
+        p = parts[i]
+        mix_sum[i].swap().wait_recv()
+        for j in range(pc.nx):
+            mm[j, p] = (mo[pc.c, j, p].astype(f32) + mp[j, p].astype(f32)).astype(bf16)
+        mix_sum[i].spread()
+
+    def norm_mid(i):
+        p = parts[i]
+        mix_sum[i].three().wait_recv()
+        mr[pc.x, p] = mm[pc.x, p]
+        mixed = sum(mr[j, p].astype(f32) for j in range(pc.nx))
+        at = pl.multiple_of(pc.t * rows + i * part_rows, part_rows)
+        res = x[pl.ds(at, part_rows)].astype(f32) + mixed.astype(bf16).astype(f32)
+        resid[p] = res
         scale = lax.rsqrt(jnp.mean(res * res, axis=-1, keepdims=True) + FLOOR)
-        nm[pc.x, pc.c] = (res * scale * mlp_gain[...]).astype(bf16)
-        norm_all.start()
+        nm[pc.t, p] = (res * scale * mlp_gain[...]).astype(bf16)
+        norm_all[i].start()
 
     def up():
-        norm_all.wait()
+        for n in norm_all:
+            n.wait()
         for k in range(last + 1):
             stream["u"].all_of(k)
             stream["v"].all_of(k)
@@ -438,7 +467,10 @@
             part = part.astype(bf16).reshape(pc.nx, 2, rows, 128)
             for core in range(2):
                 fx[g][core, :, :, pl.ds(s * 128, 128)] = part[:, core]
-        feed_sum[g].swap().start()
+        if g == end:
+            end_sum.start()
+        else:
+            feed_sum[g].swap().start()
 
     def feed_pair(g):
         feed_sum[g].swap().wait_recv()
@@ -447,43 +479,53 @@
         feed_sum[g].spread()
 
     def finish(g):
-        feed_sum[g].three().wait_recv()
-        fr[g][pc.x] = fm[g][pc.x]
+        if g == end:
+            end_sum.rest().wait_recv()
+            fr[g][pc.t] = fx[g][pc.c, pc.x]
+        else:
+            feed_sum[g].three().wait_recv()
+            fr[g][pc.x] = fm[g][pc.x]
         for s, dz in enumerate(slots(g)):
             at = pl.ds(s * 128, 128)
-            feed = sum(fr[g][i, :, at].astype(f32) for i in range(pc.nx))
+            feed = sum(fr[g][i, :, at].astype(f32) for i in range(fr[g].shape[0]))
             to = pl.ds(pl.multiple_of(pc.row(dz) * 128, 128), 128)
-            og[g][pc.x, pc.c, :, at] = (resid[:, to] + feed.astype(bf16).astype(f32)).astype(bf16)
-        feed_all[g].start()
+            og[g][pc.t, :, at] = (resid[:, to] + feed.astype(bf16).astype(f32)).astype(bf16)
+        if g == end:
+            end_all.start()
+        else:
+            feed_all[g].start()
 
     def write(g):
-        feed_all[g].wait()
+        if g == end:
+            end_all.rest().wait_recv()
+        else:
+            feed_all[g].wait()
         for s, dz in enumerate(slots(g)):
             to = pl.ds(pl.multiple_of(pc.row(dz) * 128, 128), 128)
-            pltpu.make_async_copy(og[g].at[:, :, :, pl.ds(s * 128, 128)], out.at[:, :, :, to], out_sem).start()
-
-    steps = dict(
-        N=norm_in, G=glu, C=convolve, H=channel_norm, I=lambda: mix_rows(pc.c), B=mix_pair, E=norm_mid,
-        L=norm_all.relay, U=up,
+            out[:, :, to] = og[g][:, :, pl.ds(s * 128, 128)]
+
+    steps = dict(N=norm_in, G=glu, C=convolve, H=channel_norm, I=lambda: mix_rows(pc.c), U=up)
+    by_number = dict(
+        B=mix_pair, E=norm_mid, L=lambda i: norm_all[i].relay(),
+        M=down, S=feed_pair, F=finish, R=lambda g: feed_all[g].relay(), W=write,
     )
-    by_group = dict(M=down, S=feed_pair, F=finish, R=lambda g: feed_all[g].relay(), W=write)
     for name in ORDER:
         if "." in name:
             getattr(stream[name[0]], name[2])(int(name[3:]))
         elif name in steps:
             steps[name]()
         else:
-            by_group[name[0]](int(name[1:]))
+            by_number[name[0]](int(name[1:]))
 
     for s in stream.values():
         s.drain()
-    stat_all().wait_send()
-    for s in [mix_sum, *feed_sum]:
+    for s in [stat_all, end_sum, end_all]:
+        s.rest().wait_send()
+    for s in [*mix_sum, *feed_sum]:
         s.swap().wait_send()
         s.three().wait_send()
-    for s in [norm_all, *feed_all]:
+    for s in [*norm_all, *feed_all]:
         s.drain()
-    pltpu.make_async_copy(out, out, out_sem).wait()
 
 
 def layer(nfs, nt, tok, mix_gain, vw, gw, taps, chan_gain, ow, mlp_gain, uw, dw):
@@ -500,40 +542,43 @@
     block = lambda c: pltpu.VMEM((nfs, k_rows, c), bf16)
     pairs = lambda w: pltpu.VMEM((2, nx, rows, w), bf16)
     four = lambda w: pltpu.VMEM((nx, rows, w), bf16)
-    eight = lambda w: pltpu.VMEM((nx, 2, rows, w), bf16)
-    hbm, vmem = pl.BlockSpec(memory_space=pl.ANY), pl.BlockSpec(memory_space=pltpu.VMEM)
+    eight = lambda w: pltpu.VMEM((nt, rows, w), bf16)
+    hbm, vmem = pl.BlockSpec(memory_space=pltpu.HBM), pl.BlockSpec(memory_space=pltpu.VMEM)
     scratch = [
+        pltpu.VMEM((1, width), f32), pltpu.VMEM(taps.shape, f32), pltpu.VMEM((1, wq), f32), pltpu.VMEM((1, width), f32),
         pltpu.VMEM((tokens, width), bf16),
         pltpu.VMEM((tokens, width), bf16),
         block(2 * wq), block(wq), block(uc), block(ff - uc), block(dc), block(ff - dc),
         pltpu.VMEM((wq // 128, tokens // LEN, LEN + 32, 128), f32),
         pltpu.VMEM((wq // 128, tokens, 128), f32),
         pltpu.VMEM((nt, 2, tokens), f32),
-        eight(wq),
+        pltpu.VMEM((nx, 2, rows, wq), bf16),
         pairs(width), four(width), four(width), four(width),
         eight(width),
         pltpu.VMEM((rows, width), f32),
         pltpu.VMEM((tokens, uc), bf16),
         pltpu.VMEM((tokens, ff - uc), bf16),
         [pairs(w) for w in widths], [four(w) for w in widths], [four(w) for w in widths],
-        [four(w) for w in widths], [eight(w) for w in widths],
-        dma((8,)), dma(()),
+        [*(four(w) for w in widths[:-1]), eight(widths[-1])], [eight(w) for w in widths],
+        dma((12,)),
         [z_first(), z_first(), z_first(), y_first(), z_first(), y_first()],
-        dma((2,)), dma((4,)), dma((6,)), dma((len(GROUPS), 4)), dma((len(GROUPS), 6)),
+        dma((2,)), dma((PARTS, 4)), dma((PARTS, 6)), dma((len(GROUPS), 4)), dma((len(GROUPS), 6)),
     ]
     done = pl.pallas_call(
         functools.partial(body, nfs, nt),
-        out_shape=jax.ShapeDtypeStruct((nx, 2, rows, width), bf16),
-        in_specs=[hbm, vmem, hbm, hbm, vmem, vmem, hbm, vmem, hbm, hbm],
-        out_specs=hbm,
+        out_shape=jax.ShapeDtypeStruct((nt, rows, width), bf16),
+        in_specs=[hbm] * 10,
+        out_specs=vmem,
         scratch_shapes=scratch,
         compiler_params=pltpu.CompilerParams(
-            collective_id=0, has_side_effects=True, vmem_limit_bytes=56 * 1024 * 1024
+            collective_id=0, has_side_effects=True, vmem_limit_bytes=40 * 1024 * 1024
         ),
         name="layer",
     )(
-        tok, mix_gain.reshape(1, -1), vw, gw, taps, chan_gain.reshape(1, -1), ow.T,
-        mlp_gain.reshape(1, -1), uw, dw.T,
+        *(pltpu.with_memory_space_constraint(a, pltpu.HBM) for a in (
+            tok, mix_gain.reshape(1, -1), vw, gw, taps, chan_gain.reshape(1, -1), ow.T,
+            mlp_gain.reshape(1, -1), uw, dw.T,
+        ))
     )
     return done.reshape(tokens, width)
 

time: 106 us -> 97.8 us (0.923)
  Pallas kernels: 103 us -> 96.7 us
  local copies, waits for them, and re-layouts: 2.3 us -> 0.97 us
    pallas_call x1, Pallas kernels: 103 us -> 96.7 us  [layer(): pl.pallas_call(functools.partial(body, nfs, nt), out_shape=jax.ShapeDtype...]
    unnamed x1, local copies, waits for them, and re-layouts: 2.3 us -> 0.97 us
where the time goes in v3:
time: 97.8 us; the launch traced here: 97.7 us
  Pallas kernels  96.7 us (99%)
    pallas_call x1, Pallas kernels, layer(): pl.pallas_call(functools.partial(body, nfs, nt), out_shape=jax.ShapeDtype...  96.7 us

profile of v3, /device:TPU:1, one launch (start us, length us, event | category | flops | bytes accessed | tf_op | source)
XLA Modules:
  0.0 97.7 jit_solution(13641795267386884507)
XLA Ops:
  0.0 96.7 %layer.1 = bf16[8,32,2048]{2,1,0:T(8,128)(2,1)S(1)} custom-call(bf16[256,2048]{1,0:T(8,128)(2,1)} %tok.1, f32[1,2048]{1,0:T(1,128)} %bitcast.9, bf16[32,256]{1,0:T(8,128)(2,1)} %vw.1, bf16[32,256]{1,0:T(8,128)(2,1)} %gw.1, f32[31,256]{1,0:T(8,128)} %taps_in.1, f32[1,256]{1,0:T(1,128)} %bitcast.11, bf16[32,256]{1,0:T(8,128)(2,1)} %bitcast.8, ...), custom_call_target="tpu_custom_call" | custom-call | tf_op jit(solution)/shard_map/layer/pallas_call | solution.py:567
  96.7 1.0 copy.12

commit v4 on v3

--- a/solution.py
+++ b/solution.py
@@ -14,22 +14,24 @@
 f32, bf16 = jnp.float32, jnp.bfloat16
 
 ORDER = (
-    "o.y0", "o.z0", "e.y0", "g.z0", "g.y0", "u.y0", "d.y0", "u.z0", "o.y1", "o.z1", "g.z1", "v.y0", "g.y1", "g.z2",
-    "g.y2", "g.f0", "o.z2", "v.y1", "u.z1", "o.y2", "g.z3", "g.y3", "N", "g.f1", "o.z3", "g.z4", "v.z00", "g.f2",
-    "g.y4", "o.y3", "g.z5", "g.y5", "o.z4", "g.f3", "g.z6", "u.z2", "e.y1", "g.y6", "v.z01", "g.y7", "d.z0", "o.z5",
-    "v.z10", "g.y8", "g.f4", "u.z3", "g.f5", "v.z11", "g.f6", "o.z6", "e.z00", "g.f7", "g.f8", "d.z1", "o.y5", "o.f0",
-    "o.y6", "o.y4", "o.f2", "v.z20", "o.y7", "u.y3", "o.z7", "e.z01", "G", "v.z21", "o.f5", "u.z4", "o.y8", "d.z2",
-    "u.y2", "e.z10", "o.f7", "o.f6", "v.z30", "o.f1", "C", "o.f3", "o.f4", "o.f8", "u.f3", "u.y5", "u.z5", "v.z31",
-    "u.y1", "u.y4", "d.z3", "e.z11", "v.z40", "H", "u.y6", "v.z41", "I", "u.f2", "u.z6", "B0", "u.f5", "e.z21",
-    "v.z50", "B1", "v.z51", "u.y7", "e.z20", "u.z7", "u.f4", "E0", "u.f6", "u.f0", "d.z4", "d.y2", "v.z60", "v.z61",
-    "E1", "e.z30", "u.y8", "d.z5", "d.y1", "u.f1", "e.z31", "v.z70", "L0", "u.f7", "u.f8", "v.z71", "d.f0", "d.f2",
-    "L1", "d.f1", "d.y4", "e.z40", "e.z41", "d.y3", "d.z6", "d.y6", "d.y5", "U", "e.z50", "M0", "d.f4", "e.z51",
-    "d.f3", "S0", "d.y7", "d.z7", "d.f6", "e.z60", "d.f5", "e.z61", "M1", "F0", "d.f7", "d.y8", "S1", "e.z70", "M2",
-    "e.z71", "S2", "M3", "S3", "M4", "F1", "F2", "R0", "F3", "F4", "W0", "R1", "R2", "W1", "R3", "W2", "W4", "W3",
+    "o.z0", "o.y0", "u.z0", "e.y0", "u.y0", "d.y0", "v.y0", "g.z0", "o.z1", "d.z0", "g.y0", "e.y1", "u.y1", "u.z1",
+    "g.y1", "g.z1", "v.y1", "g.y2", "o.z2", "g.z2", "o.y1", "d.z1", "u.z2", "o.y2", "o.f0", "o.z3", "u.y2", "g.y3",
+    "g.z3", "g.z4", "N", "g.y4", "o.z4", "v.z00", "v.z01", "u.z3", "u.f2", "o.f1", "g.y6", "g.z5", "g.f2", "o.z5",
+    "g.y5", "g.z6", "o.y3", "g.f0", "g.f4", "v.z11", "v.z10", "o.z6", "u.z4", "g.f1", "g.y7", "e.z00", "g.f5", "d.z2",
+    "g.f3", "g.y8", "o.y5", "v.z21", "v.z20", "o.y7", "o.z7", "e.z10", "u.z5", "g.f6", "d.z3", "o.y4", "g.f7",
+    "e.z01", "o.y8", "g.f8", "o.f3", "o.f5", "o.y6", "o.f2", "d.y1", "v.z30", "o.f7", "u.y5", "u.z6", "e.z20", "o.f8",
+    "o.f4", "G", "e.z11", "v.z31", "C", "o.f6", "u.y6", "d.y4", "d.z4", "v.z40", "u.y7", "u.y4", "e.z21", "e.z30",
+    "H", "u.z7", "I", "v.z41", "d.z5", "B0", "d.y2", "v.z50", "B1", "e.z31", "d.y3", "u.f3", "u.y8", "v.z51", "u.f4",
+    "u.f0", "u.f7", "d.y5", "u.f6", "d.y6", "u.f1", "E0", "e.z40", "v.z60", "u.f8", "u.y3", "d.f0", "d.f3", "d.z6",
+    "E1", "v.z61", "e.z41", "d.f1", "v.z70", "d.f2", "L0", "d.f5", "u.f5", "v.z71", "e.z50", "e.z51", "L1", "d.f6",
+    "d.f4", "d.y7", "d.z7", "U", "e.z60", "M0", "e.z61", "M1", "M3", "d.y8", "S0", "M2", "S3", "d.f7", "S1", "S2",
+    "e.z70", "e.z71", "F0", "M4", "F3", "S4", "M5", "F1", "F2", "R0", "R3", "F4", "W3", "F5", "R1", "R2", "W0", "R4",
+    "W1", "W2", "W5", "W4",
 )
-GROUPS = ((0, 1, 2), (3, 4), (5, 6), (7,), (8,))
+GROUPS = ((0, 1), (2, 3), (4, 5), (6,), (7,), (8,))
 STRIDE = {'g': 2}
 DIRECT = {'d': 8}
+VIA = {'u': (3, 5)}
 PARTS = 2
 
 
@@ -71,8 +73,8 @@
 
 
 class Stream:
-    def __init__(self, pc, w, sems, loads, stride, direct):
-        self.pc, self.w, self.loads, self.stride, self.direct = pc, w, loads, stride, direct
+    def __init__(self, pc, w, sems, loads, stride, direct, via):
+        self.pc, self.w, self.loads, self.stride, self.direct, self.via = pc, w, loads, stride, direct, via
         self.ss, self.zr, self.yr, self.hr = sems
         self.n = w.shape[1] // 2
         self.came = set()
@@ -111,6 +113,8 @@
                 self.await_(self.part(b, d) if k == pc.half else self.w.at[b], self.zr.at[d, k])
             elif what == "y":
                 self.await_(self.w.at[pl.ds(0, len(pc.shifts(k)))], self.yr.at[d, k])
+            elif k in self.via:
+                self.await_(self.w.at[pc.blk(k if d else -k, 2)], self.hr.at[d, k])
             elif k >= self.direct:
                 if d == 0:
                     self.await_(self.w.at[pl.ds(0, len(pc.shifts(k)))], self.hr.at[0, k])
@@ -149,6 +153,11 @@
 
     def f(self, k):
         pc = self.pc
+        if k in self.via:
+            self.need("h", k - 1)
+            for d, way in ((0, 1), (1, -1)):
+                self.send(self.w.at[pc.blk(-way * (k - 1), 2)], self.hr.at[d, k], pc.dev(way, 0))
+            return
         self.need("y", k)
         for dz in pc.shifts(k):
             for d, way in ((0, 1), (1, -1)):
@@ -303,6 +312,12 @@
     halves = wq // 128
     reach = taps.shape[0] // 2
 
+    barrier = pltpu.get_barrier_semaphore()
+    friends = [pc.dev(dz, 0) for dz in (1, -1, 2, -2)] + [pc.dev(0, dy) for dy in (1, -1, 2)]
+    friends += [(pc.f, lax.rem(pc.t + i, nt)) for i in range(1, nt)]
+    for dev in friends:
+        pl.semaphore_signal(barrier, inc=1, device_id=dev, device_id_type=MESH)
+
     def load(src, dst, i):
         copy = pltpu.make_async_copy(src, dst, load_sem.at[i])
         copy.start()
@@ -324,17 +339,12 @@
         ))
     ]
 
-    barrier = pltpu.get_barrier_semaphore()
-    friends = [pc.dev(dz, 0) for dz in (1, -1, 2, -2)] + [pc.dev(0, dy) for dy in (1, -1, 2)]
-    friends += [(pc.f, lax.rem(pc.t + i, nt)) for i in range(1, nt)]
-    for dev in friends:
-        pl.semaphore_signal(barrier, inc=1, device_id=dev, device_id_type=MESH)
     own["g"][0].wait()
     own["g"].pop(0)
     pl.semaphore_wait(barrier, len(friends))
 
     stream = {
-        name: kind(pc, w, sems[i], own[name], STRIDE.get(name, 1), DIRECT.get(name, last + 1))
+        name: kind(pc, w, sems[i], own[name], STRIDE.get(name, 1), DIRECT.get(name, last + 1), VIA.get(name, ()))
         for i, (name, kind, w) in enumerate((
             ("g", ZFirst, gb), ("o", ZFirst, ob), ("u", ZFirst, ub), ("v", YFirst, vb), ("d", ZFirst, db),
             ("e", YFirst, eb),

time: 97.8 us -> 97.6 us (level)
  no operation moved by 1% of the time
where the time goes in v4:
time: 97.6 us; the launch traced here: 97.4 us
  Pallas kernels  96.4 us (99%)
    pallas_call x1, Pallas kernels, layer(): pl.pallas_call(functools.partial(body, nfs, nt), out_shape=jax.ShapeDtype...  96.4 us

profile of v4, /device:TPU:1, one launch (start us, length us, event | category | flops | bytes accessed | tf_op | source)
XLA Modules:
  0.0 97.4 jit_solution(14450448613563576129)
XLA Ops:
  0.0 96.4 %layer.1 = bf16[8,32,2048]{2,1,0:T(8,128)(2,1)S(1)} custom-call(bf16[256,2048]{1,0:T(8,128)(2,1)} %tok.1, f32[1,2048]{1,0:T(1,128)} %bitcast.9, bf16[32,256]{1,0:T(8,128)(2,1)} %vw.1, bf16[32,256]{1,0:T(8,128)(2,1)} %gw.1, f32[31,256]{1,0:T(8,128)} %taps_in.1, f32[1,256]{1,0:T(1,128)} %bitcast.11, bf16[32,256]{1,0:T(8,128)(2,1)} %bitcast.8, ...), custom_call_target="tpu_custom_call" | custom-call | tf_op jit(solution)/shard_map/layer/pallas_call | solution.py:577
  96.4 1.0 copy.12
